TPU v7x, 32 devices: a whole 2x2x4 slice. The times are simulated.
32 devices in a mesh: sp: 16 (over z, y, x), tp: 2 (over core).
Axes of the slice: x: 2, y: 2, z: 4, core: 2. Of those that a mesh axis runs over, the one named last changes fastest.
Arguments:
- residual: bfloat16 [4096, 2048], P(('sp', 'tp')), may hold values from -6 to 6
- query_rows: bfloat16 [4096, 1024], P('sp', 'tp'), may hold values from -141 to 141
- key_rows: bfloat16 [4096, 1024], P('sp', 'tp'), may hold values from -7.8 to 7.8
- value_rows: bfloat16 [4096, 1024], P('sp', 'tp'), may hold values from -6 to 6
- mix_lambda: float32 [8], P('tp'), may hold values from 0.3 to 0.8
- documents: int32 [4096], P('sp'), may hold values from 0 to 7, never falling along the last dimension, each value on 1 to 768 neighbouring positions
- out_weight: bfloat16 [1024, 2048], replicated, may hold values from -0.1875 to 0.1875
- norm_gain: float32 [2048], replicated, may hold values from 0.1 to 1.9
- gate_weight: bfloat16 [16, 2048, 2048], P('sp', None, 'tp'), may hold values from -0.125 to 0.125
- up_weight: bfloat16 [16, 2048, 2048], P('sp', None, 'tp'), may hold values from -0.125 to 0.125
- down_weight: bfloat16 [16, 2048, 2048], P('sp', 'tp'), may hold values from -0.125 to 0.125
- routes: int32 [4096, 2], P(('sp', 'tp')), may hold values from 0 to 15, all different within a row; in each aligned block of 128 rows (0 to 127, 128 to 255, ...) at most 32 rows name the same one
- route_weights: float32 [4096, 2], P(('sp', 'tp')), may hold values from 0.25 to 1
Outputs:
- layer_out: bfloat16 [4096, 2048], P(('sp', 'tp'))
Inputs may be any that keep to these rules, and one draw needn't show every extreme that they name: `documents`: document numbers never fall along the sequence; a document covers at most 768 positions, and one covers exactly that many. `routes`: each row names two different experts. Among the rows of one index of sp+tp, no expert is named by more than 32 rows, and in every draw some expert is named by exactly 32 rows of some such block.
All inputs are finite; a program needn't handle non-finite values.
Results may differ from a plain program's by a relative error of at most 0.013.
Values may be sent and summed in bfloat16 or wider, within the bound.
A program may use at most 128 MiB of HBM per device.

v0:
```python
import jax
import jax.numpy as jnp
from jax import lax
from jax.sharding import PartitionSpec as P

HD = 64
REACH = 3


def shifted(value, axis, steps):
    count = lax.axis_size(axis)
    first, last = (max(0, -steps), min(count, count - steps))
    return lax.ppermute(value, axis, [(source, source + steps) for source in range(first, last)])


def neighbour(pieces, offset):
    return shifted((pieces[0], pieces[1], pieces[2]), "sp", offset)


def slot_order(route_block, experts):
    flat_routes = route_block.reshape(-1)
    table = (flat_routes[:, None] == jnp.arange(experts, dtype=jnp.int32)[None, :]).astype(
        jnp.int32
    )
    earlier = jnp.cumsum(table, axis=0) - table
    return (flat_routes, jnp.sum(earlier * table, axis=1))


def head_attention(same_document, score_scale):

    def attend(operands):
        head_query, head_keys, head_values, second_weight = operands
        scores = (
            jnp.einsum("qcd,kcd->cqk", head_query, head_keys, preferred_element_type=jnp.float32)
            * score_scale
        )
        masked = jnp.where(same_document[None], scores, -1e30)
        largest = jnp.max(masked, axis=-1, keepdims=True)
        lifted = jnp.exp(masked - largest)
        probabilities = lifted / jnp.sum(lifted, axis=-1, keepdims=True)
        weights = (probabilities[0] - second_weight * probabilities[1]).astype(jnp.bfloat16)
        head_out = jnp.dot(weights, head_values, preferred_element_type=jnp.float32)
        scaled = head_out * lax.rsqrt(jnp.mean(head_out * head_out, axis=-1, keepdims=True) + 1e-06)
        return scaled.astype(jnp.bfloat16)

    return attend


def on_device(
    residual,
    query_rows,
    key_rows,
    value_rows,
    mix_lambda,
    documents,
    out_weight,
    norm_gain,
    gate_weight,
    up_weight,
    down_weight,
    routes,
    route_weights,
):
    length = query_rows.shape[0]
    local_heads = mix_lambda.shape[0]
    value_dim = value_rows.shape[1] // local_heads
    model_width = residual.shape[1]
    own_ids = documents + 1
    key_parts, value_parts, id_parts = ([key_rows], [value_rows], [own_ids])
    for distance in range(1, REACH + 1):
        for offset in (distance, -distance):
            far_keys, far_values, far_ids = neighbour((key_rows, value_rows, own_ids), offset)
            key_parts.append(far_keys)
            value_parts.append(far_values)
            id_parts.append(far_ids)
    all_keys = jnp.concatenate(key_parts, axis=0).reshape(-1, local_heads, 2, HD)
    all_values = jnp.concatenate(value_parts, axis=0).reshape(-1, local_heads, value_dim)
    all_ids = jnp.concatenate(id_parts, axis=0)
    same_document = own_ids[:, None] == all_ids[None, :]
    queries = query_rows.reshape(length, local_heads, 2, HD)
    per_head = lax.map(
        head_attention(same_document, HD ** (-0.5)),
        (
            jnp.moveaxis(queries, 1, 0),
            jnp.moveaxis(all_keys, 1, 0),
            jnp.moveaxis(all_values, 1, 0),
            mix_lambda,
        ),
    )
    merged = jnp.moveaxis(per_head, 0, 1).reshape(length, local_heads * value_dim)
    token_heads = lax.all_to_all(merged, "tp", split_axis=0, concat_axis=1, tiled=True)
    projected = jnp.dot(token_heads, out_weight, preferred_element_type=jnp.float32)
    mixed = (residual.astype(jnp.float32) + projected).astype(jnp.bfloat16)
    mixed_wide = mixed.astype(jnp.float32)
    normed = (
        mixed_wide
        * lax.rsqrt(jnp.mean(mixed_wide * mixed_wide, axis=-1, keepdims=True) + 1e-06)
        * norm_gain
    ).astype(jnp.bfloat16)
    experts = lax.axis_size("sp")
    capacity = 2 * length // experts
    top_count = routes.shape[1]
    flat_routes, slot_rank = slot_order(routes, experts)
    target_rows = flat_routes * capacity + slot_rank
    sources_all = jnp.repeat(normed, top_count, axis=0)
    outgoing = jnp.zeros((experts * capacity, model_width), jnp.bfloat16)
    outgoing = outgoing.at[target_rows].set(sources_all).reshape(experts, capacity, model_width)
    arrived = lax.all_to_all(outgoing, "sp", split_axis=0, concat_axis=0, tiled=True)
    rows_all = lax.all_gather(arrived.reshape(-1, model_width), "tp", axis=0, tiled=True)
    gate = jnp.dot(rows_all, gate_weight[0], preferred_element_type=jnp.float32)
    upward = jnp.dot(rows_all, up_weight[0], preferred_element_type=jnp.float32)
    hidden = (jax.nn.silu(gate) * upward).astype(jnp.bfloat16)
    summed = lax.psum_scatter(
        jnp.dot(hidden, down_weight[0], preferred_element_type=jnp.float32).astype(jnp.bfloat16),
        "tp",
        scatter_dimension=0,
        tiled=True,
    )
    answer = summed.reshape(arrived.shape[0], arrived.shape[1], model_width)
    returned = lax.all_to_all(answer, "sp", split_axis=0, concat_axis=0, tiled=True)
    picked = returned.reshape(experts * capacity, model_width)[target_rows]
    picked = picked.reshape(-1, top_count, model_width).astype(jnp.float32)
    weighted = jnp.sum(picked * route_weights[:, :, None], axis=1)
    return (mixed_wide + weighted).astype(jnp.bfloat16)


def solution(mesh):
    placed = (
        P(("sp", "tp"), None),
        P("sp", "tp"),
        P("sp", "tp"),
        P("sp", "tp"),
        P("tp"),
        P("sp"),
        P(),
        P(),
        P("sp", None, "tp"),
        P("sp", None, "tp"),
        P("sp", "tp", None),
        P(("sp", "tp"), None),
        P(("sp", "tp"), None),
    )
    return jax.shard_map(
        on_device, mesh=mesh, in_specs=placed, out_specs=P(("sp", "tp"), None), check_vma=False
    )
```

profile of v0, /device:TPU:0, one launch (start us, length us, event | category | flops | bytes accessed | tf_op | source)
XLA Modules:
  0.0 329.0 jit_solution(15591114638349226413)
XLA Ops:
  7.3 4.9 %collective-permute-start = (s32[256]{0:T(256)S(1)}, s32[256]{0:T(256)S(1)}, u32[]{:S(2)}, u32[]{:S(2)}) collective-permute-start(s32[256]{0:T(256)S(1)} %get-tuple-element.167), channel_id=1, source_target_pairs={{0,2},{2,4},{4,6},{6,8},{8,10},{10,12},{12,14},{14,16},{16,18},{18... | collective-permute-start | bytes 3080 | tf_op jit(solution)/shard_map/ppermute | solution.py:13
  12.1 1.3 collective-permute-start.1
  13.4 5.5 %collective-permute-start.2 = (s32[256]{0:T(256)S(1)}, s32[256]{0:T(256)S(1)}, u32[]{:S(2)}, u32[]{:S(2)}) collective-permute-start(s32[256]{0:T(256)S(1)} %get-tuple-element.167), channel_id=1, source_target_pairs={{0,4},{2,6},{4,8},{6,10},{8,12},{10,14},{12,16},{14,18},{16,20},{1... | collective-permute-start | bytes 3080 | tf_op jit(solution)/shard_map/ppermute | solution.py:13
  18.9 1.3 collective-permute-start.3
  20.2 4.6 %collective-permute-start.4 = (s32[256]{0:T(256)S(1)}, s32[256]{0:T(256)S(1)}, u32[]{:S(2)}, u32[]{:S(2)}) collective-permute-start(s32[256]{0:T(256)S(1)} %get-tuple-element.167), channel_id=1, source_target_pairs={{0,6},{2,8},{4,10},{6,12},{8,14},{10,16},{12,18},{14,20},{16,22},{... | collective-permute-start | bytes 3080 | tf_op jit(solution)/shard_map/ppermute | solution.py:13
  30.7 1.3 collective-permute-start.5
  32.0 5.2 %collective-permute-start.12 = (bf16[256,512]{0,1:T(8,128)(2,1)S(1)}, bf16[256,512]{0,1:T(8,128)(2,1)S(1)}, u32[]{:S(2)}, u32[]{:S(2)}) collective-permute-start(bf16[256,512]{0,1:T(8,128)(2,1)S(1)} %copy.40), channel_id=1, source_target_pairs={{0,2},{2,4},{4,6},{6,8},{8,10},{10,12},{12,14},{14,16},{16,18},{18... | collective-permute-start | bytes 786440 | tf_op jit(solution)/shard_map/ppermute | solution.py:13
  37.3 1.3 collective-permute-start.13
  38.6 4.6 %collective-permute-start.14 = (bf16[256,512]{0,1:T(8,128)(2,1)S(1)}, bf16[256,512]{0,1:T(8,128)(2,1)S(1)}, u32[]{:S(2)}, u32[]{:S(2)}) collective-permute-start(bf16[256,512]{0,1:T(8,128)(2,1)S(1)} %copy.40), channel_id=1, source_target_pairs={{0,4},{2,6},{4,8},{6,10},{8,12},{10,14},{12,16},{14,18},{16,20},{1... | collective-permute-start | bytes 786440 | tf_op jit(solution)/shard_map/ppermute | solution.py:13
  43.2 1.3 collective-permute-start.15
  44.5 7.0 %collective-permute-start.16 = (bf16[256,512]{0,1:T(8,128)(2,1)S(1)}, bf16[256,512]{0,1:T(8,128)(2,1)S(1)}, u32[]{:S(2)}, u32[]{:S(2)}) collective-permute-start(bf16[256,512]{0,1:T(8,128)(2,1)S(1)} %copy.40), channel_id=1, source_target_pairs={{0,6},{2,8},{4,10},{6,12},{8,14},{10,16},{12,18},{14,20},{16,22},{... | collective-permute-start | bytes 786440 | tf_op jit(solution)/shard_map/ppermute | solution.py:13
  51.5 5.7 %collective-permute-start.6 = (bf16[256,512]{1,0:T(8,128)(2,1)S(1)}, bf16[256,512]{1,0:T(8,128)(2,1)S(1)}, u32[]{:S(2)}, u32[]{:S(2)}) collective-permute-start(bf16[256,512]{1,0:T(8,128)(2,1)S(1)} %copy-done.2), channel_id=1, source_target_pairs={{0,2},{2,4},{4,6},{6,8},{8,10},{10,12},{12,14},{14,16},{16,18},{18... | collective-permute-start | bytes 786440 | tf_op jit(solution)/shard_map/ppermute | solution.py:13
  60.1 4.0 %collective-permute-start.8 = (bf16[256,512]{1,0:T(8,128)(2,1)S(1)}, bf16[256,512]{1,0:T(8,128)(2,1)S(1)}, u32[]{:S(2)}, u32[]{:S(2)}) collective-permute-start(bf16[256,512]{1,0:T(8,128)(2,1)S(1)} %copy-done.2), channel_id=1, source_target_pairs={{0,4},{2,6},{4,8},{6,10},{8,12},{10,14},{12,16},{14,18},{16,20},{1... | collective-permute-start | bytes 786440 | tf_op jit(solution)/shard_map/ppermute | solution.py:13
  64.8 5.7 %collective-permute-done.6 = bf16[256,512]{1,0:T(8,128)(2,1)S(1)} collective-permute-done((bf16[256,512]{1,0:T(8,128)(2,1)S(1)}, bf16[256,512]{1,0:T(8,128)(2,1)S(1)}, u32[]{:S(2)}, u32[]{:S(2)}) %collective-permute-start.6) | collective-permute-done | bytes 262176 | tf_op jit(solution)/shard_map/ppermute | solution.py:13
  71.8 10.7 %collective-permute-start.10 = (bf16[256,512]{1,0:T(8,128)(2,1)S(1)}, bf16[256,512]{1,0:T(8,128)(2,1)S(1)}, u32[]{:S(2)}, u32[]{:S(2)}) collective-permute-start(bf16[256,512]{1,0:T(8,128)(2,1)S(1)} %copy-done.2), channel_id=1, source_target_pairs={{0,6},{2,8},{4,10},{6,12},{8,14},{10,16},{12,18},{14,20},{16,22},{... | collective-permute-start | bytes 786440 | tf_op jit(solution)/shard_map/ppermute | solution.py:13
  82.6 1.3 collective-permute-start.11
  83.9 1.3 collective-permute-start.17
  85.2 4.8 %collective-permute-done.10 = bf16[256,512]{1,0:T(8,128)(2,1)S(1)} collective-permute-done((bf16[256,512]{1,0:T(8,128)(2,1)S(1)}, bf16[256,512]{1,0:T(8,128)(2,1)S(1)}, u32[]{:S(2)}, u32[]{:S(2)}) %collective-permute-start.10) | collective-permute-done | bytes 262176 | tf_op jit(solution)/shard_map/ppermute | solution.py:13
  90.0 14.1 %collective-permute-done.11 = bf16[256,512]{1,0:T(8,128)(2,1)S(1)} collective-permute-done((bf16[256,512]{1,0:T(8,128)(2,1)S(1)}, bf16[256,512]{1,0:T(8,128)(2,1)S(1)}, u32[]{:S(2)}, u32[]{:S(2)}) %collective-permute-start.11) | collective-permute-done | bytes 262176 | tf_op jit(solution)/shard_map/ppermute | solution.py:13
  104.2 2.5 copy.33
  108.2 1.7 constant_dynamic-update-slice_fusion.7
  109.9 40.1 %while.11 = (s32[]{:T(128)}, bf16[4,256,128]{1,2,0:T(8,128)(2,1)S(1)}, bf16[4,256,2,64]{1,3,2,0:T(8,128)(2,1)S(1)}, bf16[4,1792,2,64]{1,3,2,0:T(8,128)(2,1)}, f3...) while((s32[]{:T(128)}, ...), condition=%wide.region_4.5_spmd.clone, body=%wide.region_0.4_spmd.clone.sunk | while | flops 241436672 | bytes 16926828 | solution.py:81
  110.2 4.2 %exponential_reduce_fusion.2 = (f32[2,256]{1,0:T(2,128)S(1)}, f32[2,256,1792]{2,1,0:T(8,128)}) fusion(pred[256,1792]{1,0:T(8,128)(4,1)S(1)} %broadcast_compare_fusion.2, bf16[4,1792,2,64]{1,3,2,0:T(8,128)(2,1)} %get-tuple-element.181, s32[]{:T(128)} %get-tuple-element.169, bf16[4,256,2,64]{1,3,2,0:T(8,128)(2,1)S(1)} %get-tuple-element.180), kind=kOutput, calls=%fused_computation.7.clone.1 | convolution fusion | flops 121112320 | bytes 4656128 | tf_op jit(solution)/shard_map/while/body/eval_jaxpr/sub | solution.py:39
  114.4 2.6 exponential_divide_fusion.2
  117.7 2.2 multiply_reduce_fusion.4
  120.3 4.2 %exponential_reduce_fusion.2 = (f32[2,256]{1,0:T(2,128)S(1)}, f32[2,256,1792]{2,1,0:T(8,128)}) fusion(pred[256,1792]{1,0:T(8,128)(4,1)S(1)} %broadcast_compare_fusion.2, bf16[4,1792,2,64]{1,3,2,0:T(8,128)(2,1)} %get-tuple-element.181, s32[]{:T(128)} %get-tuple-element.169, bf16[4,256,2,64]{1,3,2,0:T(8,128)(2,1)S(1)} %get-tuple-element.180), kind=kOutput, calls=%fused_computation.7.clone.1 | convolution fusion | flops 121112320 | bytes 4656128 | tf_op jit(solution)/shard_map/while/body/eval_jaxpr/sub | solution.py:39
  124.5 2.6 exponential_divide_fusion.2
  127.7 2.2 multiply_reduce_fusion.4
  130.3 4.2 %exponential_reduce_fusion.2 = (f32[2,256]{1,0:T(2,128)S(1)}, f32[2,256,1792]{2,1,0:T(8,128)}) fusion(pred[256,1792]{1,0:T(8,128)(4,1)S(1)} %broadcast_compare_fusion.2, bf16[4,1792,2,64]{1,3,2,0:T(8,128)(2,1)} %get-tuple-element.181, s32[]{:T(128)} %get-tuple-element.169, bf16[4,256,2,64]{1,3,2,0:T(8,128)(2,1)S(1)} %get-tuple-element.180), kind=kOutput, calls=%fused_computation.7.clone.1 | convolution fusion | flops 121112320 | bytes 4656128 | tf_op jit(solution)/shard_map/while/body/eval_jaxpr/sub | solution.py:39
  134.5 2.6 exponential_divide_fusion.2
  137.7 2.2 multiply_reduce_fusion.4
  140.3 4.2 %exponential_reduce_fusion.2 = (f32[2,256]{1,0:T(2,128)S(1)}, f32[2,256,1792]{2,1,0:T(8,128)}) fusion(pred[256,1792]{1,0:T(8,128)(4,1)S(1)} %broadcast_compare_fusion.2, bf16[4,1792,2,64]{1,3,2,0:T(8,128)(2,1)} %get-tuple-element.181, s32[]{:T(128)} %get-tuple-element.169, bf16[4,256,2,64]{1,3,2,0:T(8,128)(2,1)S(1)} %get-tuple-element.180), kind=kOutput, calls=%fused_computation.7.clone.1 | convolution fusion | flops 121112320 | bytes 4656128 | tf_op jit(solution)/shard_map/while/body/eval_jaxpr/sub | solution.py:39
  144.5 2.6 exponential_divide_fusion.2
  147.8 2.2 multiply_reduce_fusion.4
  150.3 3.9 %all_to_all.29 = bf16[2,128,512]{2,1,0:T(8,128)(2,1)S(1)} all-to-all(bf16[2,128,512]{2,1,0:T(8,128)(2,1)S(1)} %copy.49), channel_id=1, replica_groups=mesh['sp'=16,'tp'=2] {'tp'}, dimensions={0} | all-to-all | bytes 524288 | tf_op jit(solution)/shard_map/all_to_all | solution.py:91
  154.4 3.0 multiply_reduce_fusion.2
  159.5 3.5 %scatter_custom_fusion = bf16[512,2048]{1,0:T(8,128)(2,1)S(1)} fusion(s32[256]{0:T(256)S(1)} %bitcast.114, bf16[256,2048]{1,0:T(8,128)(2,1)} %reshape.124, bf16[]{:T(256)} %constant.23.clone.1), kind=kCustom, calls=%fused_computation.48 | custom fusion | bytes 2097664 | tf_op jit(solution)/shard_map/scatter | solution.py:107
  163.0 55.3 %all_to_all.30 = bf16[16,32,2048]{2,1,0:T(8,128)(2,1)} all-to-all(bf16[16,32,2048]{2,1,0:T(8,128)(2,1)S(1)} %bitcast.106), channel_id=1, replica_groups=mesh['sp'=16,'tp'=2] {'sp'}, dimensions={0} | all-to-all | bytes 4194304 | tf_op jit(solution)/shard_map/all_to_all | solution.py:108
  218.6 11.9 %all-gather.2.cloned.1.call-done = bf16[1024,2048]{1,0:T(8,128)(2,1)} async-done(((bf16[512,2048]{1,0:T(8,128)(2,1)}), bf16[1024,2048]{1,0:T(8,128)(2,1)}) %all-gather.2.cloned.1.call-update) | async-done | bytes 4194320 | tf_op jit(solution)/shard_map/all_gather | solution.py:109
  230.5 7.7 %fusion.36 = f32[1024,1024]{1,0:T(8,128)S(1)} fusion(bf16[1024,2048]{1,0:T(8,128)(2,1)} %all-gather.2.cloned.1.call-done, bf16[1,2048,1024]{2,1,0:T(8,128)(2,1)} %param.24), kind=kOutput, calls=%fused_computation.35 | convolution fusion | flops 4294967296 | bytes 12582912 | tf_op jit(solution)/shard_map/dot_general | solution.py:111
  238.2 5.4 %multiply_convert_fusion.1 = bf16[1024,1024]{1,0:T(8,128)(2,1)S(1)} fusion(f32[1024,1024]{1,0:T(8,128)S(1)} %fusion.36, bf16[1024,2048]{1,0:T(8,128)(2,1)S(1)} %copy-done.7, bf16[1,2048,1024]{2,1,0:T(8,128)(2,1)S(1)} %copy-done.5), kind=kOutput, calls=%fused_computation.39 | convolution fusion | flops 4301258752 | bytes 14680064 | tf_op jit(solution)/shard_map/dot_general | solution.py:110
  243.6 6.1 %fusion.40 = bf16[1024,2048]{1,0:T(8,128)(2,1)} fusion(bf16[1024,1024]{1,0:T(8,128)(2,1)S(1)} %multiply_convert_fusion.1, bf16[1,1024,2048]{2,1,0:T(8,128)(2,1)S(1)} %copy-done.6), kind=kOutput, calls=%fused_computation.40 | convolution fusion | flops 4297064448 | bytes 10485760 | tf_op jit(solution)/shard_map/dot_general | solution.py:114
  249.7 13.3 %reduce-scatter.2.cloned.1.call-done = bf16[512,2048]{1,0:T(8,128)(2,1)} async-done(((bf16[1024,2048]{1,0:T(8,128)(2,1)}), bf16[512,2048]{1,0:T(8,128)(2,1)}) %reduce-scatter.2.cloned.1.call-update) | async-done | bytes 2097168 | tf_op jit(solution)/shard_map/reduce_scatter | solution.py:113
  263.1 7.1 %all-to-all-start.2 = ((bf16[16,32,2048]{2,1,0:T(8,128)(2,1)}), bf16[16,32,2048]{2,1,0:T(8,128)(2,1)S(1)}, u32[]{:S(2)}, u32[]{:S(2)}) async-start(bf16[16,32,2048]{2,1,0:T(8,128)(2,1)} %bitcast.107), calls=%async_computation.3 | async-start | bytes 4194304 | tf_op jit(solution)/shard_map/all_to_all | solution.py:120
  270.2 43.1 %all-to-all-done.2 = bf16[16,32,2048]{2,1,0:T(8,128)(2,1)S(1)} async-done(((bf16[16,32,2048]{2,1,0:T(8,128)(2,1)}), bf16[16,32,2048]{2,1,0:T(8,128)(2,1)S(1)}, u32[]{:S(2)}, u32[]{:S(2)}) %all-to-all-start.2) | async-done | bytes 2097184 | tf_op jit(solution)/shard_map/all_to_all | solution.py:120
  313.4 2.3 gather_fusion
  315.7 2.4 reshape.111
  318.1 3.2 multiply_reduce_fusion.1
  (102 shorter events, 20.9 us)
Async XLA Ops:
  6.5 45.0 %copy-start.2 = (bf16[256,512]{1,0:T(8,128)(2,1)S(1)}, bf16[256,512]{1,0:T(8,128)(2,1)}, u32[]{:S(2)}) copy-start(bf16[256,512]{1,0:T(8,128)(2,1)} %param.17) | copy-start | bytes 786436
  6.5 24.0 %copy-start.1 = (bf16[256,512]{1,0:T(8,128)(2,1)S(1)}, bf16[256,512]{1,0:T(8,128)(2,1)}, u32[]{:S(2)}) copy-start(bf16[256,512]{1,0:T(8,128)(2,1)} %param.16) | copy-start | bytes 786436
  6.5 223.9 %all-gather.2.cloned.1.call-start = ((), (), s32[]{:S(2)}) async-start(), calls=%async_computation.4 | async-start | bytes 6291456 | tf_op jit(solution)/shard_map/all_gather | solution.py:109
  7.3 23.4 %collective-permute-start = (s32[256]{0:T(256)S(1)}, s32[256]{0:T(256)S(1)}, u32[]{:S(2)}, u32[]{:S(2)}) collective-permute-start(s32[256]{0:T(256)S(1)} %get-tuple-element.167), channel_id=1, source_target_pairs={{0,2},{2,4},{4,6},{6,8},{8,10},{10,12},{12,14},{14,16},{16,18},{18... | collective-permute-start | bytes 3080 | tf_op jit(solution)/shard_map/ppermute | solution.py:13
  12.1 19.9 %collective-permute-start.1 = (s32[256]{0:T(256)S(1)}, s32[256]{0:T(256)S(1)}, u32[]{:S(2)}, u32[]{:S(2)}) collective-permute-start(s32[256]{0:T(256)S(1)} %get-tuple-element.167), channel_id=1, source_target_pairs={{2,0},{4,2},{6,4},{8,6},{10,8},{12,10},{14,12},{16,14},{18,16},{20... | collective-permute-start | bytes 3080 | tf_op jit(solution)/shard_map/ppermute | solution.py:13
  13.4 23.8 %collective-permute-start.2 = (s32[256]{0:T(256)S(1)}, s32[256]{0:T(256)S(1)}, u32[]{:S(2)}, u32[]{:S(2)}) collective-permute-start(s32[256]{0:T(256)S(1)} %get-tuple-element.167), channel_id=1, source_target_pairs={{0,4},{2,6},{4,8},{6,10},{8,12},{10,14},{12,16},{14,18},{16,20},{1... | collective-permute-start | bytes 3080 | tf_op jit(solution)/shard_map/ppermute | solution.py:13
  18.9 19.7 %collective-permute-start.3 = (s32[256]{0:T(256)S(1)}, s32[256]{0:T(256)S(1)}, u32[]{:S(2)}, u32[]{:S(2)}) collective-permute-start(s32[256]{0:T(256)S(1)} %get-tuple-element.167), channel_id=1, source_target_pairs={{4,0},{6,2},{8,4},{10,6},{12,8},{14,10},{16,12},{18,14},{20,16},{2... | collective-permute-start | bytes 3080 | tf_op jit(solution)/shard_map/ppermute | solution.py:13
  20.2 23.0 %collective-permute-start.4 = (s32[256]{0:T(256)S(1)}, s32[256]{0:T(256)S(1)}, u32[]{:S(2)}, u32[]{:S(2)}) collective-permute-start(s32[256]{0:T(256)S(1)} %get-tuple-element.167), channel_id=1, source_target_pairs={{0,6},{2,8},{4,10},{6,12},{8,14},{10,16},{12,18},{14,20},{16,22},{... | collective-permute-start | bytes 3080 | tf_op jit(solution)/shard_map/ppermute | solution.py:13
  30.7 13.8 %collective-permute-start.5 = (s32[256]{0:T(256)S(1)}, s32[256]{0:T(256)S(1)}, u32[]{:S(2)}, u32[]{:S(2)}) collective-permute-start(s32[256]{0:T(256)S(1)} %get-tuple-element.167), channel_id=1, source_target_pairs={{6,0},{8,2},{10,4},{12,6},{14,8},{16,10},{18,12},{20,14},{22,16},{... | collective-permute-start | bytes 3080 | tf_op jit(solution)/shard_map/ppermute | solution.py:13
  32.0 19.5 %collective-permute-start.12 = (bf16[256,512]{0,1:T(8,128)(2,1)S(1)}, bf16[256,512]{0,1:T(8,128)(2,1)S(1)}, u32[]{:S(2)}, u32[]{:S(2)}) collective-permute-start(bf16[256,512]{0,1:T(8,128)(2,1)S(1)} %copy.40), channel_id=1, source_target_pairs={{0,2},{2,4},{4,6},{6,8},{8,10},{10,12},{12,14},{14,16},{16,18},{18... | collective-permute-start | bytes 786440 | tf_op jit(solution)/shard_map/ppermute | solution.py:13
  37.3 20.7 %collective-permute-start.13 = (bf16[256,512]{0,1:T(8,128)(2,1)S(1)}, bf16[256,512]{0,1:T(8,128)(2,1)S(1)}, u32[]{:S(2)}, u32[]{:S(2)}) collective-permute-start(bf16[256,512]{0,1:T(8,128)(2,1)S(1)} %copy.40), channel_id=1, source_target_pairs={{2,0},{4,2},{6,4},{8,6},{10,8},{12,10},{14,12},{16,14},{18,16},{20... | collective-permute-start | bytes 786440 | tf_op jit(solution)/shard_map/ppermute | solution.py:13
  38.6 21.4 %collective-permute-start.14 = (bf16[256,512]{0,1:T(8,128)(2,1)S(1)}, bf16[256,512]{0,1:T(8,128)(2,1)S(1)}, u32[]{:S(2)}, u32[]{:S(2)}) collective-permute-start(bf16[256,512]{0,1:T(8,128)(2,1)S(1)} %copy.40), channel_id=1, source_target_pairs={{0,4},{2,6},{4,8},{6,10},{8,12},{10,14},{12,16},{14,18},{16,20},{1... | collective-permute-start | bytes 786440 | tf_op jit(solution)/shard_map/ppermute | solution.py:13
  43.2 63.5 %collective-permute-start.15 = (bf16[256,512]{0,1:T(8,128)(2,1)S(1)}, bf16[256,512]{0,1:T(8,128)(2,1)S(1)}, u32[]{:S(2)}, u32[]{:S(2)}) collective-permute-start(bf16[256,512]{0,1:T(8,128)(2,1)S(1)} %copy.40), channel_id=1, source_target_pairs={{4,0},{6,2},{8,4},{10,6},{12,8},{14,10},{16,12},{18,14},{20,16},{2... | collective-permute-start | bytes 786440 | tf_op jit(solution)/shard_map/ppermute | solution.py:13
  44.5 62.9 %collective-permute-start.16 = (bf16[256,512]{0,1:T(8,128)(2,1)S(1)}, bf16[256,512]{0,1:T(8,128)(2,1)S(1)}, u32[]{:S(2)}, u32[]{:S(2)}) collective-permute-start(bf16[256,512]{0,1:T(8,128)(2,1)S(1)} %copy.40), channel_id=1, source_target_pairs={{0,6},{2,8},{4,10},{6,12},{8,14},{10,16},{12,18},{14,20},{16,22},{... | collective-permute-start | bytes 786440 | tf_op jit(solution)/shard_map/ppermute | solution.py:13
  51.5 18.9 %collective-permute-start.6 = (bf16[256,512]{1,0:T(8,128)(2,1)S(1)}, bf16[256,512]{1,0:T(8,128)(2,1)S(1)}, u32[]{:S(2)}, u32[]{:S(2)}) collective-permute-start(bf16[256,512]{1,0:T(8,128)(2,1)S(1)} %copy-done.2), channel_id=1, source_target_pairs={{0,2},{2,4},{4,6},{6,8},{8,10},{10,12},{12,14},{14,16},{16,18},{18... | collective-permute-start | bytes 786440 | tf_op jit(solution)/shard_map/ppermute | solution.py:13
  58.0 13.8 %collective-permute-start.7 = (bf16[256,512]{1,0:T(8,128)(2,1)S(1)}, bf16[256,512]{1,0:T(8,128)(2,1)S(1)}, u32[]{:S(2)}, u32[]{:S(2)}) collective-permute-start(bf16[256,512]{1,0:T(8,128)(2,1)S(1)} %copy-done.2), channel_id=1, source_target_pairs={{2,0},{4,2},{6,4},{8,6},{10,8},{12,10},{14,12},{16,14},{18,16},{20... | collective-permute-start | bytes 786440 | tf_op jit(solution)/shard_map/ppermute | solution.py:13
  60.1 22.5 %collective-permute-start.8 = (bf16[256,512]{1,0:T(8,128)(2,1)S(1)}, bf16[256,512]{1,0:T(8,128)(2,1)S(1)}, u32[]{:S(2)}, u32[]{:S(2)}) collective-permute-start(bf16[256,512]{1,0:T(8,128)(2,1)S(1)} %copy-done.2), channel_id=1, source_target_pairs={{0,4},{2,6},{4,8},{6,10},{8,12},{10,14},{12,16},{14,18},{16,20},{1... | collective-permute-start | bytes 786440 | tf_op jit(solution)/shard_map/ppermute | solution.py:13
  70.5 13.4 %collective-permute-start.9 = (bf16[256,512]{1,0:T(8,128)(2,1)S(1)}, bf16[256,512]{1,0:T(8,128)(2,1)S(1)}, u32[]{:S(2)}, u32[]{:S(2)}) collective-permute-start(bf16[256,512]{1,0:T(8,128)(2,1)S(1)} %copy-done.2), channel_id=1, source_target_pairs={{4,0},{6,2},{8,4},{10,6},{12,8},{14,10},{16,12},{18,14},{20,16},{2... | collective-permute-start | bytes 786440 | tf_op jit(solution)/shard_map/ppermute | solution.py:13
  71.8 18.2 %collective-permute-start.10 = (bf16[256,512]{1,0:T(8,128)(2,1)S(1)}, bf16[256,512]{1,0:T(8,128)(2,1)S(1)}, u32[]{:S(2)}, u32[]{:S(2)}) collective-permute-start(bf16[256,512]{1,0:T(8,128)(2,1)S(1)} %copy-done.2), channel_id=1, source_target_pairs={{0,6},{2,8},{4,10},{6,12},{8,14},{10,16},{12,18},{14,20},{16,22},{... | collective-permute-start | bytes 786440 | tf_op jit(solution)/shard_map/ppermute | solution.py:13
  82.6 21.6 %collective-permute-start.11 = (bf16[256,512]{1,0:T(8,128)(2,1)S(1)}, bf16[256,512]{1,0:T(8,128)(2,1)S(1)}, u32[]{:S(2)}, u32[]{:S(2)}) collective-permute-start(bf16[256,512]{1,0:T(8,128)(2,1)S(1)} %copy-done.2), channel_id=1, source_target_pairs={{6,0},{8,2},{10,4},{12,6},{14,8},{16,10},{18,12},{20,14},{22,16},{... | collective-permute-start | bytes 786440 | tf_op jit(solution)/shard_map/ppermute | solution.py:13
  83.9 24.3 %collective-permute-start.17 = (bf16[256,512]{0,1:T(8,128)(2,1)S(1)}, bf16[256,512]{0,1:T(8,128)(2,1)}, u32[]{:S(2)}, u32[]{:S(2)}) collective-permute-start(bf16[256,512]{0,1:T(8,128)(2,1)S(1)} %copy.40), channel_id=1, source_target_pairs={{6,0},{8,2},{10,4},{12,6},{14,8},{16,10},{18,12},{20,14},{22,16},{... | collective-permute-start | bytes 786440 | tf_op jit(solution)/shard_map/ppermute | solution.py:13
  104.2 5.7 %copy-start.8 = (f32[4]{0:T(128)S(1)}, f32[4]{0:T(128)}, u32[]{:S(2)}) copy-start(f32[4]{0:T(128)} %param.19) | copy-start | bytes 52
  150.0 4.4 %copy-start = (bf16[128,2048]{1,0:T(8,128)(2,1)S(1)}, bf16[128,2048]{1,0:T(8,128)(2,1)}, u32[]{:S(2)}) copy-start(bf16[128,2048]{1,0:T(8,128)(2,1)} %param.15) | copy-start | bytes 1572868
  154.4 3.0 copy-start.3
  218.3 44.7 %reduce-scatter.2.cloned.1.call-start = ((), (), s32[]{:S(2)}) async-start(), calls=%async_computation.5 | async-start | bytes 6291456 | tf_op jit(solution)/shard_map/reduce_scatter | solution.py:113
  230.5 7.7 %copy-start.5 = (bf16[1,2048,1024]{2,1,0:T(8,128)(2,1)S(1)}, bf16[1,2048,1024]{2,1,0:T(8,128)(2,1)}, u32[]{:S(2)}) copy-start(bf16[1,2048,1024]{2,1,0:T(8,128)(2,1)} %param.23) | copy-start | bytes 12582916
  230.5 7.7 %copy-start.7 = (bf16[1024,2048]{1,0:T(8,128)(2,1)S(1)}, bf16[1024,2048]{1,0:T(8,128)(2,1)}, u32[]{:S(2)}) copy-start(bf16[1024,2048]{1,0:T(8,128)(2,1)} %all-gather.2.cloned.1.call-done) | copy-start | bytes 12582916
  238.2 5.4 %copy-start.6 = (bf16[1,1024,2048]{2,1,0:T(8,128)(2,1)S(1)}, bf16[1,1024,2048]{2,1,0:T(8,128)(2,1)}, u32[]{:S(2)}) copy-start(bf16[1,1024,2048]{2,1,0:T(8,128)(2,1)} %param.25) | copy-start | bytes 12582916
  263.0 7.1 %copy-start.4 = (f32[128,2]{0,1:T(2,128)S(1)}, f32[128,2]{0,1:T(2,128)}, u32[]{:S(2)}) copy-start(f32[128,2]{0,1:T(2,128)} %param.27) | copy-start | bytes 3076
  263.1 50.3 %all-to-all-start.2 = ((bf16[16,32,2048]{2,1,0:T(8,128)(2,1)}), bf16[16,32,2048]{2,1,0:T(8,128)(2,1)S(1)}, u32[]{:S(2)}, u32[]{:S(2)}) async-start(bf16[16,32,2048]{2,1,0:T(8,128)(2,1)} %bitcast.107), calls=%async_computation.3 | async-start | bytes 4194304 | tf_op jit(solution)/shard_map/all_to_all | solution.py:120
Sparse Core Ops, SparseCore 0:
  218.5 11.9 all-gather.1
  249.8 13.1 reduce-scatter.1
where the time goes:
time: 334 us; the launch traced here: 329 us
  waiting for transfers between devices  93 us (28%)
  starting transfers between devices  71 us (21%)
  blocking collectives  59.3 us (18%)
  matrix products  47.7 us (14%)
  local copies, waits for them, and re-layouts  25.8 us (8%)
  other arithmetic  18.1 us (5%)
  between operations  13.9 us (4%)
    ppermute x18, starting transfers between devices, shifted(): lax.ppermute(value, axis, [(source, source + steps) for source in range(f...  63.7 us
    all_to_all x1, blocking collectives, on_device(): lax.all_to_all(outgoing, 'sp', split_axis=0, concat_axis=0, tiled=True)  55.3 us
    all_to_all x1, waiting for transfers between devices, on_device(): lax.all_to_all(answer, 'sp', split_axis=0, concat_axis=0, tiled=True)  43.1 us
    ppermute x18, waiting for transfers between devices, shifted(): lax.ppermute(value, axis, [(source, source + steps) for source in range(f...  24.6 us
    sub x4, matrix products, attend(): lifted = jnp.exp(masked - largest)  16.8 us
    reduce_scatter x1, waiting for transfers between devices, on_device(): lax.psum_scatter(jnp.dot(hidden, down_weight[0], preferred_element_type=j...  13.3 us
    all_gather x1, waiting for transfers between devices, on_device(): lax.all_gather(arrived.reshape(-1, model_width), 'tp', axis=0, tiled=True)  11.9 us
    div x4, other arithmetic, attend(): probabilities = lifted / jnp.sum(lifted, axis=-1, keepdims=True)  10.3 us
  transfers between devices with their start and end apart: 21, of which 6 were waited for; matrix products, arithmetic and copies ran while one was open for 4% of the time, Pallas kernels for 0%

commit v1 on v0

v1 whole, which is shorter than its diff:
```python
import functools

import jax
import jax.numpy as jnp
from jax import lax
from jax.experimental import pallas as pl
from jax.experimental.pallas import tpu as pltpu
from jax.sharding import PartitionSpec as P

HD = 64
REACH = 3
MESH = pl.DeviceIdType.MESH
VMEM = pl.BlockSpec(memory_space=pltpu.VMEM)


def offsets_of(reach):
    return [sign * step for step in range(1, reach + 1) for sign in (1, -1)]


def halo_kernel(count, k_ref, v_ref, id_ref, k_out, v_out, id_out, send_sem, recv_sem):
    me, core = lax.axis_index("sp"), lax.axis_index("tp")
    offsets = offsets_of(REACH)
    barrier = pltpu.get_barrier_semaphore()

    def inside(offset):
        return jnp.logical_and(me + offset >= 0, me + offset < count)

    for offset in offsets:

        @pl.when(inside(offset))
        def _():
            pl.semaphore_signal(barrier, inc=1, device_id=(me + offset, core), device_id_type=MESH)

    pl.semaphore_wait(barrier, jnp.minimum(me, REACH) + jnp.minimum(count - 1 - me, REACH))

    def copies(at, offset):
        slot = REACH - offset
        return [
            pltpu.make_async_remote_copy(
                src_ref=source,
                dst_ref=target.at[slot],
                send_sem=send_sem.at[at, which],
                recv_sem=recv_sem.at[at, which],
                device_id=(me + offset, core),
                device_id_type=MESH,
            )
            for which, (source, target) in enumerate(
                ((id_ref, id_out), (k_ref, k_out), (v_ref, v_out))
            )
        ]

    for at, offset in enumerate(offsets):

        @pl.when(inside(offset))
        def _():
            for copy in copies(at, offset):
                copy.start()

    k_out[REACH] = k_ref[...]
    v_out[REACH] = v_ref[...]
    id_out[REACH] = id_ref[...]
    for offset in offsets:

        @pl.when(jnp.logical_not(inside(-offset)))
        def _():
            slot = REACH - offset
            k_out[slot] = jnp.zeros_like(k_ref)
            v_out[slot] = jnp.zeros_like(v_ref)
            id_out[slot] = jnp.full_like(id_ref, -1)

    for at, offset in enumerate(offsets):

        @pl.when(inside(-offset))
        def _():
            for copy in copies(at, offset):
                copy.wait_recv()

    for at, offset in enumerate(offsets):

        @pl.when(inside(offset))
        def _():
            for copy in copies(at, offset):
                copy.wait_send()


def halo(count, key_rows, value_rows, ids):
    slots = 2 * REACH + 1
    outs = [
        jax.ShapeDtypeStruct((slots,) + part.shape, part.dtype)
        for part in (key_rows, value_rows, ids)
    ]
    return pl.pallas_call(
        functools.partial(halo_kernel, count),
        out_shape=outs,
        in_specs=[VMEM] * 3,
        out_specs=[VMEM] * 3,
        scratch_shapes=[
            pltpu.SemaphoreType.DMA((2 * REACH, 3)),
            pltpu.SemaphoreType.DMA((2 * REACH, 3)),
        ],
        compiler_params=pltpu.CompilerParams(collective_id=0, has_side_effects=True),
        name="halo",
    )(key_rows, value_rows, ids)


def attention_kernel(lambda_ref, q_ref, k_ref, v_ref, own_ref, all_ref, out_ref):
    head = pl.program_id(0)
    query = q_ref[...]
    lane = lax.broadcasted_iota(jnp.int32, query.shape, 1)
    same = own_ref[...] == all_ref[...]
    scale = jnp.asarray(HD ** (-0.5), query.dtype)
    contract = (((1,), (1,)), ((), ()))

    def lifted(keep):
        part = jnp.where(keep, query * scale, jnp.zeros_like(query))
        scores = lax.dot_general(part, k_ref[...], contract, preferred_element_type=jnp.float32)
        masked = jnp.where(same, scores, -1e30)
        powers = jnp.exp(masked - jnp.max(masked, axis=-1, keepdims=True))
        return powers, jnp.sum(powers, axis=-1, keepdims=True)

    first, first_sum = lifted(lane < HD)
    second, second_sum = lifted(lane >= HD)
    weights = first * (1.0 / first_sum) - second * (lambda_ref[head] / second_sum)
    head_out = jnp.dot(
        weights.astype(jnp.bfloat16), v_ref[...], preferred_element_type=jnp.float32
    )
    scaled = head_out * lax.rsqrt(jnp.mean(head_out * head_out, axis=-1, keepdims=True) + 1e-06)
    out_ref[...] = scaled.astype(jnp.bfloat16)


def attention(query_rows, all_keys, all_values, own_ids, all_ids, mix_lambda):
    length, width = query_rows.shape
    heads = mix_lambda.shape[0]
    wide, keys = width // heads, all_keys.shape[0]
    value_dim = all_values.shape[1] // heads
    rows = min(length, 128)
    return pl.pallas_call(
        attention_kernel,
        grid=(heads, length // rows),
        out_shape=jax.ShapeDtypeStruct((length, heads * value_dim), jnp.bfloat16),
        in_specs=[
            pl.BlockSpec(memory_space=pltpu.SMEM),
            pl.BlockSpec((rows, wide), lambda h, r: (r, h)),
            pl.BlockSpec((keys, wide), lambda h, r: (0, h)),
            pl.BlockSpec((keys, value_dim), lambda h, r: (0, h)),
            pl.BlockSpec((rows, 1), lambda h, r: (r, 0)),
            pl.BlockSpec((1, keys), lambda h, r: (0, 0)),
        ],
        out_specs=pl.BlockSpec((rows, value_dim), lambda h, r: (r, h)),
        name="attention",
    )(mix_lambda, query_rows, all_keys, all_values, own_ids, all_ids)


def greet_all(count, me, core):
    barrier = pltpu.get_barrier_semaphore()
    pl.semaphore_signal(barrier, inc=1, device_id=(me, 1 - core), device_id_type=MESH)

    @pl.loop(1, count)
    def _(step):
        pl.semaphore_signal(
            barrier, inc=1, device_id=((me + step) % count, core), device_id_type=MESH
        )

    pl.semaphore_wait(barrier, count)


def dispatch_kernel(count, out_ref, rows_ref, send_sem, recv_sem, pass_sem, come_sem, own_sem):
    me, core = lax.axis_index("sp"), lax.axis_index("tp")
    greet_all(count, me, core)

    def across(step):
        target = (me + step) % count
        return pltpu.make_async_remote_copy(
            src_ref=out_ref.at[target],
            dst_ref=rows_ref.at[core, me],
            send_sem=send_sem.at[step],
            recv_sem=recv_sem.at[step],
            device_id=(target, core),
            device_id_type=MESH,
        )

    def arrived(step):
        source = (me - step + count) % count
        return pltpu.make_async_remote_copy(
            src_ref=rows_ref.at[core, source],
            dst_ref=rows_ref.at[core, source],
            send_sem=pass_sem.at[step],
            recv_sem=recv_sem.at[step],
            device_id=(me, 1 - core),
            device_id_type=MESH,
        )

    def beside(step, side, source_ref=None):
        source = (me - step + count) % count
        return pltpu.make_async_remote_copy(
            src_ref=rows_ref.at[side, source] if source_ref is None else source_ref,
            dst_ref=rows_ref.at[side, source],
            send_sem=pass_sem.at[step],
            recv_sem=come_sem.at[step],
            device_id=(me, 1 - core),
            device_id_type=MESH,
        )

    @pl.loop(1, count)
    def _(step):
        across(step).start()

    own = pltpu.make_async_copy(out_ref.at[me], rows_ref.at[core, me], own_sem)
    own.start()
    beside(0, core, out_ref.at[me]).start()

    @pl.loop(1, count)
    def _(step):
        arrived(step).wait_recv()
        beside(step, core).start()

    own.wait()

    @pl.loop(0, count)
    def _(step):
        beside(step, 1 - core).wait_recv()
        beside(step, core).wait_send()

    @pl.loop(1, count)
    def _(step):
        across(step).wait_send()


def dispatch(count, outgoing):
    return pl.pallas_call(
        functools.partial(dispatch_kernel, count),
        out_shape=jax.ShapeDtypeStruct((2,) + outgoing.shape, outgoing.dtype),
        in_specs=[VMEM],
        out_specs=VMEM,
        scratch_shapes=[pltpu.SemaphoreType.DMA((count,))] * 4 + [pltpu.SemaphoreType.DMA],
        compiler_params=pltpu.CompilerParams(collective_id=1, has_side_effects=True),
        name="dispatch",
    )(outgoing)


def give_back_kernel(
    count, part_ref, back_ref, far_ref, sum_ref, pass_sem, come_sem, send_sem, recv_sem
):
    me, core = lax.axis_index("sp"), lax.axis_index("tp")
    greet_all(count, me, core)

    def beside(step):
        at = (me + step) % count
        return pltpu.make_async_remote_copy(
            src_ref=part_ref.at[1 - core, at],
            dst_ref=far_ref.at[at],
            send_sem=pass_sem.at[step],
            recv_sem=come_sem.at[step],
            device_id=(me, 1 - core),
            device_id_type=MESH,
        )

    def across(step):
        target = (me + step) % count
        return pltpu.make_async_remote_copy(
            src_ref=sum_ref.at[target],
            dst_ref=back_ref.at[me],
            send_sem=send_sem.at[step],
            recv_sem=recv_sem.at[step],
            device_id=(target, core),
            device_id_type=MESH,
        )

    def arrived(step):
        source = (me - step + count) % count
        return pltpu.make_async_remote_copy(
            src_ref=sum_ref.at[source],
            dst_ref=back_ref.at[source],
            send_sem=send_sem.at[step],
            recv_sem=recv_sem.at[step],
            device_id=(source, core),
            device_id_type=MESH,
        )

    def total(step):
        at = (me + step) % count
        beside(step).wait_recv()
        own = part_ref[core, at].astype(jnp.float32)
        return (own + far_ref[at].astype(jnp.float32)).astype(sum_ref.dtype), at

    @pl.loop(1, count)
    def _(step):
        beside(step).start()

    beside(0).start()

    @pl.loop(1, count)
    def _(step):
        value, at = total(step)
        sum_ref[at] = value

        @pl.when(step > 1)
        def _():
            across(step - 1).start()

    value, at = total(0)
    back_ref[at] = value
    across(count - 1).start()

    @pl.loop(1, count)
    def _(step):
        arrived(step).wait_recv()
        across(step).wait_send()

    @pl.loop(0, count)
    def _(step):
        beside(step).wait_send()


def give_back(count, partial):
    shape = partial.shape[1:]
    return pl.pallas_call(
        functools.partial(give_back_kernel, count),
        out_shape=jax.ShapeDtypeStruct(shape, partial.dtype),
        in_specs=[VMEM],
        out_specs=VMEM,
        scratch_shapes=[pltpu.VMEM(shape, partial.dtype)] * 2
        + [pltpu.SemaphoreType.DMA((count,))] * 4,
        compiler_params=pltpu.CompilerParams(collective_id=2, has_side_effects=True),
        name="give_back",
    )(partial)


def slots_of(routes, experts, capacity):
    flat_routes = routes.reshape(-1)
    table = (flat_routes[:, None] == jnp.arange(experts, dtype=jnp.int32)[None, :]).astype(
        jnp.float32
    )
    count = table.shape[0]
    before = jnp.tril(jnp.ones((count, count), jnp.bfloat16), -1)
    earlier = jnp.dot(before, table.astype(jnp.bfloat16), preferred_element_type=jnp.float32)
    rank = jnp.sum(earlier * table, axis=1).astype(jnp.int32)
    return (flat_routes * capacity + rank).reshape(routes.shape)


def on_device(
    residual,
    query_rows,
    key_rows,
    value_rows,
    mix_lambda,
    documents,
    out_weight,
    norm_gain,
    gate_weight,
    up_weight,
    down_weight,
    routes,
    route_weights,
):
    length = query_rows.shape[0]
    model_width = residual.shape[1]
    experts = lax.axis_size("sp")
    capacity = 2 * length // experts
    top_count = routes.shape[1]
    keys, values, ids = halo(experts, key_rows, value_rows, documents.reshape(1, length))
    merged = attention(
        query_rows,
        keys.reshape(-1, keys.shape[-1]),
        values.reshape(-1, values.shape[-1]),
        documents.reshape(length, 1),
        ids.reshape(1, -1),
        mix_lambda,
    )
    token_heads = lax.all_to_all(merged, "tp", split_axis=0, concat_axis=1, tiled=True)
    projected = jnp.dot(token_heads, out_weight, preferred_element_type=jnp.float32)
    mixed = (residual.astype(jnp.float32) + projected).astype(jnp.bfloat16)
    mixed_wide = mixed.astype(jnp.float32)
    normed = (
        mixed_wide
        * lax.rsqrt(jnp.mean(mixed_wide * mixed_wide, axis=-1, keepdims=True) + 1e-06)
        * norm_gain
    ).astype(jnp.bfloat16)
    slots = slots_of(routes, experts, capacity)
    places = jnp.arange(experts * capacity, dtype=jnp.int32)
    spread = jnp.any(slots[None, :, :] == places[:, None, None], axis=-1).astype(jnp.bfloat16)
    outgoing = jnp.dot(spread, normed, preferred_element_type=jnp.float32).astype(jnp.bfloat16)
    rows_all = dispatch(experts, outgoing.reshape(experts, capacity, model_width))
    shape = rows_all.shape
    rows_all = rows_all.reshape(-1, model_width)
    gate = jnp.dot(rows_all, gate_weight[0], preferred_element_type=jnp.float32)
    upward = jnp.dot(rows_all, up_weight[0], preferred_element_type=jnp.float32)
    hidden = (jax.nn.silu(gate) * upward).astype(jnp.bfloat16)
    partial = jnp.dot(hidden, down_weight[0], preferred_element_type=jnp.float32).astype(
        jnp.bfloat16
    )
    returned = give_back(experts, partial.reshape(shape)).reshape(-1, model_width)
    weighted = 0.0
    for which in range(top_count):
        pick = (slots[:, which][:, None] == places[None, :]).astype(jnp.bfloat16)
        picked = jnp.dot(pick, returned, preferred_element_type=jnp.float32)
        weighted = weighted + picked * route_weights[:, which][:, None]
    return (mixed_wide + weighted).astype(jnp.bfloat16)


def solution(mesh):
    placed = (
        P(("sp", "tp"), None),
        P("sp", "tp"),
        P("sp", "tp"),
        P("sp", "tp"),
        P("tp"),
        P("sp"),
        P(),
        P(),
        P("sp", None, "tp"),
        P("sp", None, "tp"),
        P("sp", "tp", None),
        P(("sp", "tp"), None),
        P(("sp", "tp"), None),
    )
    return jax.shard_map(
        on_device, mesh=mesh, in_specs=placed, out_specs=P(("sp", "tp"), None), check_vma=False
    )
```

time: 334 us -> 228 us (0.68)
  the two profiles are of different devices: /device:TPU:0 before, /device:TPU:15 now
where the time goes in v1:
time: 228 us
  Pallas kernels  190 us (83%)
  matrix products  28.4 us (12%)
  starting transfers between devices  4.96 us (2%)
  local copies, waits for them, and re-layouts  3.81 us (2%)
    pallas_call x1, Pallas kernels, dispatch(): pl.pallas_call(functools.partial(dispatch_kernel, count), out_shape=jax.S...  69 us
    pallas_call x1, Pallas kernels, give_back(): pl.pallas_call(functools.partial(give_back_kernel, count), out_shape=jax....  60.4 us
    pallas_call x1, Pallas kernels, halo(): pl.pallas_call(functools.partial(halo_kernel, count), out_shape=outs, in_...  49.9 us
    pallas_call x1, Pallas kernels, attention(): pl.pallas_call(attention_kernel, grid=(heads, length // rows), out_shape=...  11 us
    dot_general x1, matrix products, on_device(): upward = jnp.dot(rows_all, up_weight[0], preferred_element_type=jnp.float32)  7.97 us
    dot_general x1, matrix products, on_device(): jnp.dot(hidden, down_weight[0], preferred_element_type=jnp.float32)  6.07 us
    dot_general x1, matrix products, on_device(): gate = jnp.dot(rows_all, gate_weight[0], preferred_element_type=jnp.float32)  5.35 us
    all_to_all x1, starting transfers between devices, on_device(): lax.all_to_all(merged, 'tp', split_axis=0, concat_axis=1, tiled=True)  4.96 us
  transfers between devices with their start and end apart: 1, of which 1 were waited for; matrix products, arithmetic and copies ran while one was open for 0% of the time, Pallas kernels for 0%

profile of v1, /device:TPU:15, one launch (start us, length us, event | category | flops | bytes accessed | tf_op | source)
XLA Modules:
  0.0 228.0 jit_solution(3777103568396039154)
XLA Ops:
  0.0 0.0 copy-start.4
  0.0 0.0 copy-start.2
  0.0 1.5 copy.31.own_ref
  1.5 49.9 %halo.1 = (bf16[7,256,512]{2,1,0:T(8,128)(2,1)}, bf16[7,256,512]{2,1,0:T(8,128)(2,1)}, s32[7,1,256]{2,1,0:T(1,128)}) custom-call(bf16[256,512]{1,0:T(8,128)(2,1)} %k_ref.1, bf16[256,512]{1,0:T(8,128)(2,1)} %v_ref.1, s32[1,256]{1,0:T(1,128)} %bitcast.54), custom_call_target="tpu_custom_call" | custom-call | tf_op jit(solution)/shard_map/halo/pallas_call | solution.py:92
  51.4 11.0 %attention.1 = bf16[256,512]{1,0:T(8,128)(2,1)} custom-call(f32[4]{0:T(128)} %lambda_ref.1, bf16[256,512]{1,0:T(8,128)(2,1)} %q_ref.1, bf16[1792,512]{1,0:T(8,128)(2,1)} %bitcast.48, bf16[1792,512]{1,0:T(8,128)(2,1)} %bitcast.49, s32[256,1]{1,0:T(8,128)} %copy.31.own_ref, s32[1,1792]{1,0:T(1,128)} %bitcast.52), custom_call_target="tpu_custom_call" | custom-call | tf_op jit(solution)/shard_map/attention/pallas_call | solution.py:137
  62.4 0.0 copy-start.3
  62.4 1.8 copy.32
  64.2 5.0 %all-to-all-start = ((bf16[2,128,512]{1,2,0:T(8,128)(2,1)}), bf16[2,128,512]{1,2,0:T(8,128)(2,1)S(1)}, u32[]{:S(2)}, u32[]{:S(2)}) async-start(bf16[2,128,512]{1,2,0:T(8,128)(2,1)} %copy.32), calls=%async_computation | async-start | bytes 524288 | tf_op jit(solution)/shard_map/all_to_all | solution.py:370
  69.2 0.0 copy-done.4
  69.2 0.1 copy.33
  69.3 0.1 eq.58
  69.4 0.3 fusion.16
  69.7 0.1 convert_element_type.48
  69.8 0.1 copy.34
  69.9 0.1 fusion.19
  70.0 0.3 all-to-all-done
  70.3 0.0 copy-done.2
  70.4 3.0 %multiply_reduce_fusion = (f32[128]{0:T(128)S(1)}, f32[128,2048]{1,0:T(8,128)S(1)}) fusion(bf16[128,1024]{0,1:T(8,128)(2,1)S(1)} %bitcast.50, bf16[1024,2048]{1,0:T(8,128)(2,1)} %param.19, bf16[128,2048]{1,0:T(8,128)(2,1)S(1)} %copy-done.2), kind=kOutput, calls=%fused_computation.20 | convolution fusion | flops 538443648 | bytes 6029824 | tf_op jit(solution)/shard_map/dot_general | solution.py:371
  73.4 0.0 copy-done.3
  73.4 2.1 convolution_convert_fusion
  75.5 69.0 %dispatch.1 = bf16[2,16,32,2048]{3,2,1,0:T(8,128)(2,1)} custom-call(bf16[16,32,2048]{2,1,0:T(8,128)(2,1)} %bitcast.44), custom_call_target="tpu_custom_call" | custom-call | tf_op jit(solution)/shard_map/dispatch/pallas_call | solution.py:230
  144.5 0.0 copy-start.1
  144.5 0.0 copy-start.6
  144.5 8.0 %fusion.2 = f32[1024,1024]{1,0:T(8,128)S(1)} fusion(bf16[1024,2048]{1,0:T(8,128)(2,1)} %bitcast.45, bf16[1,2048,1024]{2,1,0:T(8,128)(2,1)} %param.22), kind=kOutput, calls=%fused_computation.2 | convolution fusion | flops 4294967296 | bytes 12582912 | tf_op jit(solution)/shard_map/dot_general | solution.py:387
  152.5 0.0 copy-done.1
  152.5 0.0 copy-done.6
  152.5 0.0 copy-start.7
  152.5 5.4 %multiply_convert_fusion = bf16[1024,1024]{1,0:T(8,128)(2,1)S(1)} fusion(f32[1024,1024]{1,0:T(8,128)S(1)} %fusion.2, bf16[1024,2048]{1,0:T(8,128)(2,1)S(1)} %bitcast.46, bf16[1,2048,1024]{2,1,0:T(8,128)(2,1)S(1)} %copy-done.6), kind=kOutput, calls=%fused_computation.6 | convolution fusion | flops 4301258752 | bytes 14680064 | tf_op jit(solution)/shard_map/dot_general | solution.py:386
  157.8 0.0 copy-done.7
  157.9 6.1 %fusion.6 = bf16[1024,2048]{1,0:T(8,128)(2,1)} fusion(bf16[1024,1024]{1,0:T(8,128)(2,1)S(1)} %multiply_convert_fusion, bf16[1,1024,2048]{2,1,0:T(8,128)(2,1)S(1)} %copy-done.7), kind=kOutput, calls=%fused_computation.7 | convolution fusion | flops 4297064448 | bytes 10485760 | tf_op jit(solution)/shard_map/dot_general | solution.py:389
  163.9 0.0 copy-start.5
  163.9 60.4 %give_back.1 = bf16[16,32,2048]{2,1,0:T(8,128)(2,1)} custom-call(bf16[2,16,32,2048]{3,2,1,0:T(8,128)(2,1)} %bitcast.47), custom_call_target="tpu_custom_call" | custom-call | tf_op jit(solution)/shard_map/give_back/pallas_call | solution.py:317
  224.3 0.0 copy-done.5
  224.3 0.0 copy-start
  224.4 2.2 convolution_multiply_fusion.1
  226.6 0.0 copy-done
  226.6 1.4 fusion.15
  (6 shorter events, 0.0 us)
Async XLA Ops:
  0.0 69.2 %copy-start.4 = (s32[128,2]{0,1:T(2,128)S(1)}, s32[128,2]{0,1:T(2,128)}, u32[]{:S(2)}) copy-start(s32[128,2]{0,1:T(2,128)} %param.24) | copy-start | bytes 3076
  0.0 70.3 %copy-start.2 = (bf16[128,2048]{1,0:T(8,128)(2,1)S(1)}, bf16[128,2048]{1,0:T(8,128)(2,1)}, u32[]{:S(2)}) copy-start(bf16[128,2048]{1,0:T(8,128)(2,1)} %param.13) | copy-start | bytes 1572868
  62.4 11.0 %copy-start.3 = (f32[2048]{0:T(1024)S(1)}, f32[2048]{0:T(1024)}, u32[]{:S(2)}) copy-start(f32[2048]{0:T(1024)} %param.20) | copy-start | bytes 24580
  64.2 6.2 %all-to-all-start = ((bf16[2,128,512]{1,2,0:T(8,128)(2,1)}), bf16[2,128,512]{1,2,0:T(8,128)(2,1)S(1)}, u32[]{:S(2)}, u32[]{:S(2)}) async-start(bf16[2,128,512]{1,2,0:T(8,128)(2,1)} %copy.32), calls=%async_computation | async-start | bytes 524288 | tf_op jit(solution)/shard_map/all_to_all | solution.py:370
  144.5 8.0 %copy-start.1 = (bf16[2,16,32,2048]{3,2,1,0:T(8,128)(2,1)S(1)}, bf16[2,16,32,2048]{3,2,1,0:T(8,128)(2,1)}, u32[]{:S(2)}) copy-start(bf16[2,16,32,2048]{3,2,1,0:T(8,128)(2,1)} %dispatch.1) | copy-start | bytes 12582916
  144.5 8.0 %copy-start.6 = (bf16[1,2048,1024]{2,1,0:T(8,128)(2,1)S(1)}, bf16[1,2048,1024]{2,1,0:T(8,128)(2,1)}, u32[]{:S(2)}) copy-start(bf16[1,2048,1024]{2,1,0:T(8,128)(2,1)} %param.21) | copy-start | bytes 12582916
  152.5 5.4 %copy-start.7 = (bf16[1,1024,2048]{2,1,0:T(8,128)(2,1)S(1)}, bf16[1,1024,2048]{2,1,0:T(8,128)(2,1)}, u32[]{:S(2)}) copy-start(bf16[1,1024,2048]{2,1,0:T(8,128)(2,1)} %param.23) | copy-start | bytes 12582916
  163.9 60.4 %copy-start.5 = (f32[128,2]{0,1:T(2,128)S(1)}, f32[128,2]{0,1:T(2,128)}, u32[]{:S(2)}) copy-start(f32[128,2]{0,1:T(2,128)} %param.25) | copy-start | bytes 3076
  224.3 2.3 copy-start

commit v2 on v1

--- a/solution.py
+++ b/solution.py
@@ -17,21 +17,32 @@
     return [sign * step for step in range(1, reach + 1) for sign in (1, -1)]
 
 
-def halo_kernel(count, k_ref, v_ref, id_ref, k_out, v_out, id_out, send_sem, recv_sem):
+def halo_kernel(
+    count, k_ref, v_ref, id_ref, k_out, v_out, id_out, send_sem, recv_sem, pass_sem
+):
     me, core = lax.axis_index("sp"), lax.axis_index("tp")
     offsets = offsets_of(REACH)
+    group = REACH + 1
     barrier = pltpu.get_barrier_semaphore()
 
     def inside(offset):
         return jnp.logical_and(me + offset >= 0, me + offset < count)
 
-    for offset in offsets:
+    for offset in offsets_of(group):
 
         @pl.when(inside(offset))
         def _():
             pl.semaphore_signal(barrier, inc=1, device_id=(me + offset, core), device_id_type=MESH)
 
-    pl.semaphore_wait(barrier, jnp.minimum(me, REACH) + jnp.minimum(count - 1 - me, REACH))
+    pl.semaphore_wait(barrier, jnp.minimum(me, group) + jnp.minimum(count - 1 - me, group))
+
+    place = me % group
+
+    def near(offset):
+        return jnp.logical_and(place + offset >= 0, place + offset < group)
+
+    def opposite(offset):
+        return place + (place + offset + group) % group == group - 1
 
     def copies(at, offset):
         slot = REACH - offset
@@ -49,9 +60,33 @@
             )
         ]
 
+    def passes(at, offset):
+        hop = group if offset < 0 else -group
+        beyond = offset + hop
+        return [
+            pltpu.make_async_remote_copy(
+                src_ref=part.at[REACH - offset],
+                dst_ref=part.at[REACH - beyond],
+                send_sem=pass_sem.at[at, which],
+                recv_sem=recv_sem.at[offsets.index(beyond), which],
+                device_id=(me + hop, core),
+                device_id_type=MESH,
+            )
+            for which, part in enumerate((id_out, k_out, v_out))
+        ]
+
+    def sends(offset):
+        return jnp.logical_and(inside(offset), jnp.logical_or(near(offset), opposite(offset)))
+
+    def relays(offset):
+        hop = group if offset < 0 else -group
+        aligned = jnp.logical_and(inside(-offset), near(-offset))
+        aligned = jnp.logical_and(aligned, jnp.logical_not(opposite(-offset)))
+        return jnp.logical_and(aligned, inside(hop))
+
     for at, offset in enumerate(offsets):
 
-        @pl.when(inside(offset))
+        @pl.when(sends(offset))
         def _():
             for copy in copies(at, offset):
                 copy.start()
@@ -68,18 +103,31 @@
             v_out[slot] = jnp.zeros_like(v_ref)
             id_out[slot] = jnp.full_like(id_ref, -1)
 
+    for which in range(3):
+        for at, offset in enumerate(offsets):
+
+            @pl.when(relays(offset))
+            def _():
+                copies(at, offset)[which].wait_recv()
+                passes(at, offset)[which].start()
+
     for at, offset in enumerate(offsets):
 
-        @pl.when(inside(-offset))
+        @pl.when(jnp.logical_and(inside(-offset), jnp.logical_not(relays(offset))))
         def _():
             for copy in copies(at, offset):
                 copy.wait_recv()
 
     for at, offset in enumerate(offsets):
 
-        @pl.when(inside(offset))
+        @pl.when(sends(offset))
         def _():
             for copy in copies(at, offset):
+                copy.wait_send()
+
+        @pl.when(relays(offset))
+        def _():
+            for copy in passes(at, offset):
                 copy.wait_send()
 
 
@@ -94,10 +142,7 @@
         out_shape=outs,
         in_specs=[VMEM] * 3,
         out_specs=[VMEM] * 3,
-        scratch_shapes=[
-            pltpu.SemaphoreType.DMA((2 * REACH, 3)),
-            pltpu.SemaphoreType.DMA((2 * REACH, 3)),
-        ],
+        scratch_shapes=[pltpu.SemaphoreType.DMA((2 * REACH, 3))] * 3,
         compiler_params=pltpu.CompilerParams(collective_id=0, has_side_effects=True),
         name="halo",
     )(key_rows, value_rows, ids)
@@ -283,24 +328,27 @@
         own = part_ref[core, at].astype(jnp.float32)
         return (own + far_ref[at].astype(jnp.float32)).astype(sum_ref.dtype), at
 
-    @pl.loop(1, count)
-    def _(step):
-        beside(step).start()
+    def far_first(turn):
+        return (turn + count // 2 - 2) % (count - 1) + 1
+
+    @pl.loop(1, count)
+    def _(turn):
+        beside(far_first(turn)).start()
 
     beside(0).start()
 
     @pl.loop(1, count)
-    def _(step):
-        value, at = total(step)
+    def _(turn):
+        value, at = total(far_first(turn))
         sum_ref[at] = value
 
-        @pl.when(step > 1)
-        def _():
-            across(step - 1).start()
+        @pl.when(turn > 1)
+        def _():
+            across(far_first(turn - 1)).start()
 
     value, at = total(0)
     back_ref[at] = value
-    across(count - 1).start()
+    across(far_first(count - 1)).start()
 
     @pl.loop(1, count)
     def _(step):

time: 228 us -> 224 us (0.982)
  the two profiles are of different devices: /device:TPU:15 before, /device:TPU:0 now
where the time goes in v2:
time: 224 us
  Pallas kernels  187 us (83%)
  matrix products  28.4 us (13%)
  local copies, waits for them, and re-layouts  3.81 us (2%)
  starting transfers between devices  3.44 us (2%)
    pallas_call x1, Pallas kernels, give_back(): pl.pallas_call(functools.partial(give_back_kernel, count), out_shape=jax....  74.7 us
    pallas_call x1, Pallas kernels, halo(): pl.pallas_call(functools.partial(halo_kernel, count), out_shape=outs, in_...  58.4 us
    pallas_call x1, Pallas kernels, dispatch(): pl.pallas_call(functools.partial(dispatch_kernel, count), out_shape=jax.S...  43.1 us
    pallas_call x1, Pallas kernels, attention(): pl.pallas_call(attention_kernel, grid=(heads, length // rows), out_shape=...  11 us
    dot_general x1, matrix products, on_device(): upward = jnp.dot(rows_all, up_weight[0], preferred_element_type=jnp.float32)  7.98 us
    dot_general x1, matrix products, on_device(): jnp.dot(hidden, down_weight[0], preferred_element_type=jnp.float32)  6.08 us
    dot_general x1, matrix products, on_device(): gate = jnp.dot(rows_all, gate_weight[0], preferred_element_type=jnp.float32)  5.36 us
  transfers between devices with their start and end apart: 1, of which 1 were waited for; matrix products, arithmetic and copies ran while one was open for 0% of the time, Pallas kernels for 0%

profile of v2, /device:TPU:0, one launch (start us, length us, event | category | flops | bytes accessed | tf_op | source)
XLA Modules:
  0.0 223.8 jit_solution(15958327870211301957)
XLA Ops:
  0.0 0.0 copy-start.4
  0.0 0.0 copy-start.2
  0.0 1.5 copy.31.own_ref
  1.5 58.4 %halo.1 = (bf16[7,256,512]{2,1,0:T(8,128)(2,1)}, bf16[7,256,512]{2,1,0:T(8,128)(2,1)}, s32[7,1,256]{2,1,0:T(1,128)}) custom-call(bf16[256,512]{1,0:T(8,128)(2,1)} %k_ref.1, bf16[256,512]{1,0:T(8,128)(2,1)} %v_ref.1, s32[1,256]{1,0:T(1,128)} %bitcast.54), custom_call_target="tpu_custom_call" | custom-call | tf_op jit(solution)/shard_map/halo/pallas_call | solution.py:140
  59.9 11.0 %attention.1 = bf16[256,512]{1,0:T(8,128)(2,1)} custom-call(f32[4]{0:T(128)} %lambda_ref.1, bf16[256,512]{1,0:T(8,128)(2,1)} %q_ref.1, bf16[1792,512]{1,0:T(8,128)(2,1)} %bitcast.48, bf16[1792,512]{1,0:T(8,128)(2,1)} %bitcast.49, s32[256,1]{1,0:T(8,128)} %copy.31.own_ref, s32[1,1792]{1,0:T(1,128)} %bitcast.52), custom_call_target="tpu_custom_call" | custom-call | tf_op jit(solution)/shard_map/attention/pallas_call | solution.py:182
  70.9 0.0 copy-start.3
  70.9 1.8 copy.32
  72.7 3.4 %all-to-all-start = ((bf16[2,128,512]{1,2,0:T(8,128)(2,1)}), bf16[2,128,512]{1,2,0:T(8,128)(2,1)S(1)}, u32[]{:S(2)}, u32[]{:S(2)}) async-start(bf16[2,128,512]{1,2,0:T(8,128)(2,1)} %copy.32), calls=%async_computation | async-start | bytes 524288 | tf_op jit(solution)/shard_map/all_to_all | solution.py:418
  76.2 0.0 copy-done.4
  76.2 0.1 copy.33
  76.3 0.1 eq.58
  76.4 0.3 fusion.16
  76.7 0.1 convert_element_type.48
  76.9 0.1 copy.34
  76.9 0.1 fusion.19
  77.0 0.7 all-to-all-done
  77.7 0.0 copy-done.2
  77.7 3.0 %multiply_reduce_fusion = (f32[128]{0:T(128)S(1)}, f32[128,2048]{1,0:T(8,128)S(1)}) fusion(bf16[128,1024]{0,1:T(8,128)(2,1)S(1)} %bitcast.50, bf16[1024,2048]{1,0:T(8,128)(2,1)} %param.19, bf16[128,2048]{1,0:T(8,128)(2,1)S(1)} %copy-done.2), kind=kOutput, calls=%fused_computation.20 | convolution fusion | flops 538443648 | bytes 6029824 | tf_op jit(solution)/shard_map/dot_general | solution.py:419
  80.7 0.0 copy-done.3
  80.7 2.1 convolution_convert_fusion
  82.8 43.1 %dispatch.1 = bf16[2,16,32,2048]{3,2,1,0:T(8,128)(2,1)} custom-call(bf16[16,32,2048]{2,1,0:T(8,128)(2,1)} %bitcast.44), custom_call_target="tpu_custom_call" | custom-call | tf_op jit(solution)/shard_map/dispatch/pallas_call | solution.py:275
  125.9 0.0 copy-start.1
  126.0 0.0 copy-start.6
  126.0 8.0 %fusion.2 = f32[1024,1024]{1,0:T(8,128)S(1)} fusion(bf16[1024,2048]{1,0:T(8,128)(2,1)} %bitcast.45, bf16[1,2048,1024]{2,1,0:T(8,128)(2,1)} %param.22), kind=kOutput, calls=%fused_computation.2 | convolution fusion | flops 4294967296 | bytes 12582912 | tf_op jit(solution)/shard_map/dot_general | solution.py:435
  134.0 0.0 copy-done.1
  134.0 0.0 copy-done.6
  134.0 0.0 copy-start.7
  134.0 5.4 %multiply_convert_fusion = bf16[1024,1024]{1,0:T(8,128)(2,1)S(1)} fusion(f32[1024,1024]{1,0:T(8,128)S(1)} %fusion.2, bf16[1024,2048]{1,0:T(8,128)(2,1)S(1)} %bitcast.46, bf16[1,2048,1024]{2,1,0:T(8,128)(2,1)S(1)} %copy-done.6), kind=kOutput, calls=%fused_computation.6 | convolution fusion | flops 4301258752 | bytes 14680064 | tf_op jit(solution)/shard_map/dot_general | solution.py:434
  139.4 0.0 copy-done.7
  139.4 6.1 %fusion.6 = bf16[1024,2048]{1,0:T(8,128)(2,1)} fusion(bf16[1024,1024]{1,0:T(8,128)(2,1)S(1)} %multiply_convert_fusion, bf16[1,1024,2048]{2,1,0:T(8,128)(2,1)S(1)} %copy-done.7), kind=kOutput, calls=%fused_computation.7 | convolution fusion | flops 4297064448 | bytes 10485760 | tf_op jit(solution)/shard_map/dot_general | solution.py:437
  145.4 0.0 copy-start.5
  145.4 74.7 %give_back.1 = bf16[16,32,2048]{2,1,0:T(8,128)(2,1)} custom-call(bf16[2,16,32,2048]{3,2,1,0:T(8,128)(2,1)} %bitcast.47), custom_call_target="tpu_custom_call" | custom-call | tf_op jit(solution)/shard_map/give_back/pallas_call | solution.py:365
  220.2 0.0 copy-done.5
  220.2 0.0 copy-start
  220.2 2.2 convolution_multiply_fusion.1
  222.4 0.0 copy-done
  222.4 1.4 fusion.15
  (6 shorter events, 0.0 us)
Async XLA Ops:
  0.0 76.2 %copy-start.4 = (s32[128,2]{0,1:T(2,128)S(1)}, s32[128,2]{0,1:T(2,128)}, u32[]{:S(2)}) copy-start(s32[128,2]{0,1:T(2,128)} %param.24) | copy-start | bytes 3076
  0.0 77.7 %copy-start.2 = (bf16[128,2048]{1,0:T(8,128)(2,1)S(1)}, bf16[128,2048]{1,0:T(8,128)(2,1)}, u32[]{:S(2)}) copy-start(bf16[128,2048]{1,0:T(8,128)(2,1)} %param.13) | copy-start | bytes 1572868
  70.9 9.8 %copy-start.3 = (f32[2048]{0:T(1024)S(1)}, f32[2048]{0:T(1024)}, u32[]{:S(2)}) copy-start(f32[2048]{0:T(1024)} %param.20) | copy-start | bytes 24580
  72.7 5.0 %all-to-all-start = ((bf16[2,128,512]{1,2,0:T(8,128)(2,1)}), bf16[2,128,512]{1,2,0:T(8,128)(2,1)S(1)}, u32[]{:S(2)}, u32[]{:S(2)}) async-start(bf16[2,128,512]{1,2,0:T(8,128)(2,1)} %copy.32), calls=%async_computation | async-start | bytes 524288 | tf_op jit(solution)/shard_map/all_to_all | solution.py:418
  125.9 8.0 %copy-start.1 = (bf16[2,16,32,2048]{3,2,1,0:T(8,128)(2,1)S(1)}, bf16[2,16,32,2048]{3,2,1,0:T(8,128)(2,1)}, u32[]{:S(2)}) copy-start(bf16[2,16,32,2048]{3,2,1,0:T(8,128)(2,1)} %dispatch.1) | copy-start | bytes 12582916
  126.0 8.0 %copy-start.6 = (bf16[1,2048,1024]{2,1,0:T(8,128)(2,1)S(1)}, bf16[1,2048,1024]{2,1,0:T(8,128)(2,1)}, u32[]{:S(2)}) copy-start(bf16[1,2048,1024]{2,1,0:T(8,128)(2,1)} %param.21) | copy-start | bytes 12582916
  134.0 5.4 %copy-start.7 = (bf16[1,1024,2048]{2,1,0:T(8,128)(2,1)S(1)}, bf16[1,1024,2048]{2,1,0:T(8,128)(2,1)}, u32[]{:S(2)}) copy-start(bf16[1,1024,2048]{2,1,0:T(8,128)(2,1)} %param.23) | copy-start | bytes 12582916
  145.4 74.7 %copy-start.5 = (f32[128,2]{0,1:T(2,128)S(1)}, f32[128,2]{0,1:T(2,128)}, u32[]{:S(2)}) copy-start(f32[128,2]{0,1:T(2,128)} %param.25) | copy-start | bytes 3076
  220.2 2.2 %copy-start = (bf16[16,32,2048]{2,1,0:T(8,128)(2,1)S(1)}, bf16[16,32,2048]{2,1,0:T(8,128)(2,1)}, u32[]{:S(2)}) copy-start(bf16[16,32,2048]{2,1,0:T(8,128)(2,1)} %give_back.1) | copy-start | bytes 6291460

commit v3 on v2

--- a/solution.py
+++ b/solution.py
@@ -209,169 +209,204 @@
     pl.semaphore_wait(barrier, count)
 
 
-def dispatch_kernel(count, out_ref, rows_ref, send_sem, recv_sem, pass_sem, come_sem, own_sem):
+def experts_kernel(
+    count,
+    out_ref,
+    gate_hbm,
+    up_hbm,
+    down_hbm,
+    back_ref,
+    rows_ref,
+    part_ref,
+    far_ref,
+    sum_ref,
+    hidden_ref,
+    gate_ref,
+    up_ref,
+    down_ref,
+    load_sem,
+    own_sem,
+    send_sem,
+    recv_sem,
+    pass_sem,
+    come_sem,
+    swap_sem,
+    half_sem,
+    give_sem,
+    take_sem,
+):
     me, core = lax.axis_index("sp"), lax.axis_index("tp")
+    per = rows_ref.shape[2]
+    groups = count // per
+    layer, place = me // per, me % per
     greet_all(count, me, core)
 
-    def across(step):
-        target = (me + step) % count
+    def ahead(g, j):
+        return (layer + g) % groups * per + (place + j) % per
+
+    def behind(g, j):
+        return (layer - g + groups) % groups * per + (place - j + per) % per
+
+    def remote(source, target, sent, came, at, side):
         return pltpu.make_async_remote_copy(
-            src_ref=out_ref.at[target],
-            dst_ref=rows_ref.at[core, me],
-            send_sem=send_sem.at[step],
-            recv_sem=recv_sem.at[step],
-            device_id=(target, core),
+            src_ref=source,
+            dst_ref=target,
+            send_sem=sent,
+            recv_sem=came,
+            device_id=(at, side),
             device_id_type=MESH,
         )
 
-    def arrived(step):
-        source = (me - step + count) % count
-        return pltpu.make_async_remote_copy(
-            src_ref=rows_ref.at[core, source],
-            dst_ref=rows_ref.at[core, source],
-            send_sem=pass_sem.at[step],
-            recv_sem=recv_sem.at[step],
-            device_id=(me, 1 - core),
-            device_id_type=MESH,
-        )
-
-    def beside(step, side, source_ref=None):
-        source = (me - step + count) % count
-        return pltpu.make_async_remote_copy(
-            src_ref=rows_ref.at[side, source] if source_ref is None else source_ref,
-            dst_ref=rows_ref.at[side, source],
-            send_sem=pass_sem.at[step],
-            recv_sem=come_sem.at[step],
-            device_id=(me, 1 - core),
-            device_id_type=MESH,
-        )
+    def across(g, j):
+        at = ahead(g, j)
+        return remote(
+            out_ref.at[at], rows_ref.at[g, core, j], send_sem.at[g, j], recv_sem.at[g, j], at, core
+        )
+
+    def forward(g, j, side):
+        block = rows_ref.at[g, side, j]
+        return remote(block, block, pass_sem.at[g, j], come_sem.at[g, j], me, 1 - core)
+
+    def swap(g):
+        return remote(
+            part_ref.at[g, 1 - core], far_ref.at[g], swap_sem.at[g], half_sem.at[g], me, 1 - core
+        )
+
+    def home(g, j):
+        at = behind(g, j)
+        return remote(
+            sum_ref.at[g, j], back_ref.at[me], give_sem.at[g, j], take_sem.at[g, j], at, core
+        )
+
+    def came_home(g, j):
+        at = ahead(g, j)
+        return remote(
+            sum_ref.at[g, j], back_ref.at[at], give_sem.at[g, j], take_sem.at[g, j], at, core
+        )
+
+    own = pltpu.make_async_copy(out_ref.at[me], rows_ref.at[0, core, 0], own_sem)
+    own.start()
 
     @pl.loop(1, count)
     def _(step):
-        across(step).start()
-
-    own = pltpu.make_async_copy(out_ref.at[me], rows_ref.at[core, me], own_sem)
-    own.start()
-    beside(0, core, out_ref.at[me]).start()
+        across(step // per, step % per).start()
+
+    loads = [
+        pltpu.make_async_copy(source, target, load_sem.at[which])
+        for which, (source, target) in enumerate(
+            ((gate_hbm, gate_ref), (up_hbm, up_ref), (down_hbm, down_ref))
+        )
+    ]
+    for load in loads:
+        load.start()
+    own.wait()
+    forward(0, 0, core).start()
+
+    @pl.loop(0, groups)
+    def _(g):
+        for j in range(per):
+
+            @pl.when(g + j > 0)
+            def _():
+                across(g, j).wait_recv()
+                forward(g, j, core).start()
+
+        for j in range(per):
+            forward(g, j, 1 - core).wait_recv()
+
+        @pl.when(g == 0)
+        def _():
+            for load in loads:
+                load.wait()
+
+        rows, width = hidden_ref.shape
+        model = down_ref.shape[1]
+        wide = min(256, width)
+
+        @pl.loop(0, width // wide)
+        def _(c):
+            cut = pl.ds(pl.multiple_of(c * wide, wide), wide)
+            taken = rows_ref[g].reshape(rows, model)
+            gate = jnp.dot(taken, gate_ref[:, cut], preferred_element_type=jnp.float32)
+            upward = jnp.dot(taken, up_ref[:, cut], preferred_element_type=jnp.float32)
+            hidden_ref[:, cut] = (gate / (1.0 + jnp.exp(-gate)) * upward).astype(hidden_ref.dtype)
+
+        @pl.loop(0, model // wide)
+        def _(c):
+            cut = pl.ds(pl.multiple_of(c * wide, wide), wide)
+            product = jnp.dot(
+                hidden_ref[...], down_ref[:, cut], preferred_element_type=jnp.float32
+            ).astype(part_ref.dtype)
+            part_ref[g, :, :, :, cut] = product.reshape(part_ref.shape[1:4] + (wide,))
+
+        swap(g).start()
+        swap(g).wait_recv()
+        for j in range(per):
+            mine = part_ref[g, core, j].astype(jnp.float32)
+            sum_ref[g, j] = (mine + far_ref[g, j].astype(jnp.float32)).astype(sum_ref.dtype)
+            if j > 0:
+
+                @pl.when(g + j > 1)
+                def _():
+                    home(g, j - 1).start()
+
+        home(g, per - 1).start()
+
+    back_ref[me] = sum_ref[0, 0]
 
     @pl.loop(1, count)
     def _(step):
-        arrived(step).wait_recv()
-        beside(step, core).start()
-
-    own.wait()
+        g, j = step // per, step % per
+        came_home(g, j).wait_recv()
+        home(g, j).wait_send()
+        across(g, j).wait_send()
 
     @pl.loop(0, count)
     def _(step):
-        beside(step, 1 - core).wait_recv()
-        beside(step, core).wait_send()
-
-    @pl.loop(1, count)
-    def _(step):
-        across(step).wait_send()
-
-
-def dispatch(count, outgoing):
+        forward(step // per, step % per, core).wait_send()
+
+    @pl.loop(0, groups)
+    def _(g):
+        swap(g).wait_send()
+
+
+def run_experts(count, outgoing, gate_weight, up_weight, down_weight):
+    _, capacity, model = outgoing.shape
+    per = REACH + 1
+    groups = count // per
+    hidden = gate_weight.shape[1]
+    kept = outgoing.dtype
+    each = pltpu.SemaphoreType.DMA((groups, per))
+    whole = pltpu.SemaphoreType.DMA((groups,))
+    anywhere = pl.BlockSpec(memory_space=pl.ANY)
     return pl.pallas_call(
-        functools.partial(dispatch_kernel, count),
-        out_shape=jax.ShapeDtypeStruct((2,) + outgoing.shape, outgoing.dtype),
-        in_specs=[VMEM],
+        functools.partial(experts_kernel, count),
+        out_shape=jax.ShapeDtypeStruct(outgoing.shape, kept),
+        in_specs=[VMEM, anywhere, anywhere, anywhere],
         out_specs=VMEM,
-        scratch_shapes=[pltpu.SemaphoreType.DMA((count,))] * 4 + [pltpu.SemaphoreType.DMA],
+        scratch_shapes=[
+            pltpu.VMEM((groups, 2, per, capacity, model), kept),
+            pltpu.VMEM((groups, 2, per, capacity, model), kept),
+            pltpu.VMEM((groups, per, capacity, model), kept),
+            pltpu.VMEM((groups, per, capacity, model), kept),
+            pltpu.VMEM((2 * per * capacity, hidden), kept),
+            pltpu.VMEM(gate_weight.shape, kept),
+            pltpu.VMEM(up_weight.shape, kept),
+            pltpu.VMEM(down_weight.shape, kept),
+            pltpu.SemaphoreType.DMA((3,)),
+            pltpu.SemaphoreType.DMA,
+            each,
+            each,
+            each,
+            each,
+            whole,
+            whole,
+            each,
+            each,
+        ],
         compiler_params=pltpu.CompilerParams(collective_id=1, has_side_effects=True),
-        name="dispatch",
-    )(outgoing)
-
-
-def give_back_kernel(
-    count, part_ref, back_ref, far_ref, sum_ref, pass_sem, come_sem, send_sem, recv_sem
-):
-    me, core = lax.axis_index("sp"), lax.axis_index("tp")
-    greet_all(count, me, core)
-
-    def beside(step):
-        at = (me + step) % count
-        return pltpu.make_async_remote_copy(
-            src_ref=part_ref.at[1 - core, at],
-            dst_ref=far_ref.at[at],
-            send_sem=pass_sem.at[step],
-            recv_sem=come_sem.at[step],
-            device_id=(me, 1 - core),
-            device_id_type=MESH,
-        )
-
-    def across(step):
-        target = (me + step) % count
-        return pltpu.make_async_remote_copy(
-            src_ref=sum_ref.at[target],
-            dst_ref=back_ref.at[me],
-            send_sem=send_sem.at[step],
-            recv_sem=recv_sem.at[step],
-            device_id=(target, core),
-            device_id_type=MESH,
-        )
-
-    def arrived(step):
-        source = (me - step + count) % count
-        return pltpu.make_async_remote_copy(
-            src_ref=sum_ref.at[source],
-            dst_ref=back_ref.at[source],
-            send_sem=send_sem.at[step],
-            recv_sem=recv_sem.at[step],
-            device_id=(source, core),
-            device_id_type=MESH,
-        )
-
-    def total(step):
-        at = (me + step) % count
-        beside(step).wait_recv()
-        own = part_ref[core, at].astype(jnp.float32)
-        return (own + far_ref[at].astype(jnp.float32)).astype(sum_ref.dtype), at
-
-    def far_first(turn):
-        return (turn + count // 2 - 2) % (count - 1) + 1
-
-    @pl.loop(1, count)
-    def _(turn):
-        beside(far_first(turn)).start()
-
-    beside(0).start()
-
-    @pl.loop(1, count)
-    def _(turn):
-        value, at = total(far_first(turn))
-        sum_ref[at] = value
-
-        @pl.when(turn > 1)
-        def _():
-            across(far_first(turn - 1)).start()
-
-    value, at = total(0)
-    back_ref[at] = value
-    across(far_first(count - 1)).start()
-
-    @pl.loop(1, count)
-    def _(step):
-        arrived(step).wait_recv()
-        across(step).wait_send()
-
-    @pl.loop(0, count)
-    def _(step):
-        beside(step).wait_send()
-
-
-def give_back(count, partial):
-    shape = partial.shape[1:]
-    return pl.pallas_call(
-        functools.partial(give_back_kernel, count),
-        out_shape=jax.ShapeDtypeStruct(shape, partial.dtype),
-        in_specs=[VMEM],
-        out_specs=VMEM,
-        scratch_shapes=[pltpu.VMEM(shape, partial.dtype)] * 2
-        + [pltpu.SemaphoreType.DMA((count,))] * 4,
-        compiler_params=pltpu.CompilerParams(collective_id=2, has_side_effects=True),
-        name="give_back",
-    )(partial)
+        name="experts",
+    )(outgoing, gate_weight, up_weight, down_weight)
 
 
 def slots_of(routes, experts, capacity):
@@ -428,16 +463,13 @@
     places = jnp.arange(experts * capacity, dtype=jnp.int32)
     spread = jnp.any(slots[None, :, :] == places[:, None, None], axis=-1).astype(jnp.bfloat16)
     outgoing = jnp.dot(spread, normed, preferred_element_type=jnp.float32).astype(jnp.bfloat16)
-    rows_all = dispatch(experts, outgoing.reshape(experts, capacity, model_width))
-    shape = rows_all.shape
-    rows_all = rows_all.reshape(-1, model_width)
-    gate = jnp.dot(rows_all, gate_weight[0], preferred_element_type=jnp.float32)
-    upward = jnp.dot(rows_all, up_weight[0], preferred_element_type=jnp.float32)
-    hidden = (jax.nn.silu(gate) * upward).astype(jnp.bfloat16)
-    partial = jnp.dot(hidden, down_weight[0], preferred_element_type=jnp.float32).astype(
-        jnp.bfloat16
-    )
-    returned = give_back(experts, partial.reshape(shape)).reshape(-1, model_width)
+    returned = run_experts(
+        experts,
+        outgoing.reshape(experts, capacity, model_width),
+        gate_weight[0],
+        up_weight[0],
+        down_weight[0],
+    ).reshape(-1, model_width)
     weighted = 0.0
     for which in range(top_count):
         pick = (slots[:, which][:, None] == places[None, :]).astype(jnp.bfloat16)

time: 224 us -> 202 us (0.902)
  matrix products: 28.4 us -> 9.05 us
  Pallas kernels: 187 us -> 184 us
    dot_general x3 -> x0, matrix products: 19.4 us -> none  [the longest x1 7.98 us: on_device(): upward = jnp.dot(rows_all, up_weight[0], preferred_element_type=jnp.float32)]
    pallas_call x2 -> x1, Pallas kernels: 118 us -> 115 us  [run_experts(): pl.pallas_call(functools.partial(experts_kernel, count), out_shape=jax.Sh...]
where the time goes in v3:
time: 202 us; the launch traced here: 201 us
  Pallas kernels  184 us (91%)
  matrix products  9.05 us (4%)
  local copies, waits for them, and re-layouts  3.73 us (2%)
  starting transfers between devices  3.44 us (2%)
    pallas_call x1, Pallas kernels, run_experts(): pl.pallas_call(functools.partial(experts_kernel, count), out_shape=jax.Sh...  115 us
    pallas_call x1, Pallas kernels, halo(): pl.pallas_call(functools.partial(halo_kernel, count), out_shape=outs, in_...  58.4 us
    pallas_call x1, Pallas kernels, attention(): pl.pallas_call(attention_kernel, grid=(heads, length // rows), out_shape=...  11.1 us
  transfers between devices with their start and end apart: 1, of which 1 were waited for; matrix products, arithmetic and copies ran while one was open for 0% of the time, Pallas kernels for 0%

profile of v3, /device:TPU:0, one launch (start us, length us, event | category | flops | bytes accessed | tf_op | source)
XLA Modules:
  0.0 201.3 jit_solution(12842373366484577460)
XLA Ops:
  0.0 1.5 copy.31.own_ref
  1.5 58.4 %halo.1 = (bf16[7,256,512]{2,1,0:T(8,128)(2,1)}, bf16[7,256,512]{2,1,0:T(8,128)(2,1)}, s32[7,1,256]{2,1,0:T(1,128)}) custom-call(bf16[256,512]{1,0:T(8,128)(2,1)} %k_ref.1, bf16[256,512]{1,0:T(8,128)(2,1)} %v_ref.1, s32[1,256]{1,0:T(1,128)} %bitcast.39), custom_call_target="tpu_custom_call" | custom-call | tf_op jit(solution)/shard_map/halo/pallas_call | solution.py:140
  59.9 0.0 copy-start.3
  59.9 0.0 copy-start.1
  59.9 11.1 %attention.1 = bf16[256,512]{1,0:T(8,128)(2,1)} custom-call(f32[4]{0:T(128)} %lambda_ref.1, bf16[256,512]{1,0:T(8,128)(2,1)} %q_ref.1, bf16[1792,512]{1,0:T(8,128)(2,1)} %bitcast.33, bf16[1792,512]{1,0:T(8,128)(2,1)} %bitcast.34, s32[256,1]{1,0:T(8,128)} %copy.31.own_ref, s32[1,1792]{1,0:T(1,128)} %bitcast.37), custom_call_target="tpu_custom_call" | custom-call | tf_op jit(solution)/shard_map/attention/pallas_call | solution.py:182
  70.9 1.8 copy.32
  72.7 3.4 %all-to-all-start = ((bf16[2,128,512]{1,2,0:T(8,128)(2,1)}), bf16[2,128,512]{1,2,0:T(8,128)(2,1)S(1)}, u32[]{:S(2)}, u32[]{:S(2)}) async-start(bf16[2,128,512]{1,2,0:T(8,128)(2,1)} %copy.32), calls=%async_computation | async-start | bytes 524288 | tf_op jit(solution)/shard_map/all_to_all | solution.py:453
  76.2 0.0 copy-done.3
  76.2 0.1 copy.33
  76.3 0.1 eq.58
  76.4 0.3 fusion.5
  76.7 0.1 convert_element_type.42
  76.9 0.1 copy.34
  76.9 0.1 fusion.8
  77.0 0.7 all-to-all-done
  77.7 0.0 copy-done.1
  77.7 0.0 copy-start.4
  77.7 0.0 copy-start.2
  77.7 3.0 %multiply_reduce_fusion = (f32[128]{0:T(128)S(1)}, f32[128,2048]{1,0:T(8,128)S(1)}) fusion(bf16[128,1024]{0,1:T(8,128)(2,1)S(1)} %bitcast.35, bf16[1024,2048]{1,0:T(8,128)(2,1)} %param.19, bf16[128,2048]{1,0:T(8,128)(2,1)S(1)} %copy-done.1), kind=kOutput, calls=%fused_computation.12 | convolution fusion | flops 538443648 | bytes 6029824 | tf_op jit(solution)/shard_map/dot_general | solution.py:454
  80.8 0.0 copy-done.4
  80.8 0.0 copy-done.2
  80.8 2.1 %convolution_convert_fusion = bf16[512,2048]{1,0:T(8,128)(2,1)} fusion(pred[512,128]{1,0:T(8,128)(4,1)S(1)} %fusion.8, f32[128,2048]{1,0:T(8,128)S(1)} %get-tuple-element.16, f32[2048]{0:T(1024)S(1)} %copy-done.2, f32[128]{0:T(128)S(1)} %add_rsqrt_fusion), kind=kOutput, calls=%fused_computation | convolution fusion | flops 270270464 | bytes 3219968 | tf_op jit(solution)/shard_map/dot_general | solution.py:465
  82.9 114.7 %experts.1 = bf16[16,32,2048]{2,1,0:T(8,128)(2,1)} custom-call(bf16[16,32,2048]{2,1,0:T(8,128)(2,1)} %bitcast.29, bf16[2048,1024]{1,0:T(8,128)(2,1)} %bitcast.30, bf16[2048,1024]{1,0:T(8,128)(2,1)} %bitcast.31, bf16[1024,2048]{1,0:T(8,128)(2,1)} %bitcast.32), custom_call_target="tpu_custom_call" | custom-call | tf_op jit(solution)/shard_map/experts/pallas_call | solution.py:382
  197.6 0.0 copy-start
  197.6 2.2 %convolution_multiply_fusion.1 = f32[128,2048]{1,0:T(8,128)S(1)} fusion(bf16[512,2048]{1,0:T(8,128)(2,1)} %bitcast.27, f32[128]{0:T(128)S(1)} %get-tuple-element.14, s32[128]{0:T(128)S(1)} %get-tuple-element.12), kind=kOutput, calls=%fused_computation.4 | convolution fusion | flops 268763136 | bytes 3146752 | tf_op jit(solution)/shard_map/dot_general | solution.py:476
  199.8 0.0 copy-done
  199.8 1.4 fusion.4
  (6 shorter events, 0.0 us)
Async XLA Ops:
  59.9 16.3 %copy-start.3 = (s32[128,2]{0,1:T(2,128)S(1)}, s32[128,2]{0,1:T(2,128)}, u32[]{:S(2)}) copy-start(s32[128,2]{0,1:T(2,128)} %param.24) | copy-start | bytes 3076
  59.9 17.8 %copy-start.1 = (bf16[128,2048]{1,0:T(8,128)(2,1)S(1)}, bf16[128,2048]{1,0:T(8,128)(2,1)}, u32[]{:S(2)}) copy-start(bf16[128,2048]{1,0:T(8,128)(2,1)} %param.13) | copy-start | bytes 1572868
  72.7 5.0 %all-to-all-start = ((bf16[2,128,512]{1,2,0:T(8,128)(2,1)}), bf16[2,128,512]{1,2,0:T(8,128)(2,1)S(1)}, u32[]{:S(2)}, u32[]{:S(2)}) async-start(bf16[2,128,512]{1,2,0:T(8,128)(2,1)} %copy.32), calls=%async_computation | async-start | bytes 524288 | tf_op jit(solution)/shard_map/all_to_all | solution.py:453
  77.7 3.1 %copy-start.4 = (f32[128,2]{0,1:T(2,128)S(1)}, f32[128,2]{0,1:T(2,128)}, u32[]{:S(2)}) copy-start(f32[128,2]{0,1:T(2,128)} %param.25) | copy-start | bytes 3076
  77.7 3.1 %copy-start.2 = (f32[2048]{0:T(1024)S(1)}, f32[2048]{0:T(1024)}, u32[]{:S(2)}) copy-start(f32[2048]{0:T(1024)} %param.20) | copy-start | bytes 24580
  197.6 2.2 %copy-start = (bf16[16,32,2048]{2,1,0:T(8,128)(2,1)S(1)}, bf16[16,32,2048]{2,1,0:T(8,128)(2,1)}, u32[]{:S(2)}) copy-start(bf16[16,32,2048]{2,1,0:T(8,128)(2,1)} %experts.1) | copy-start | bytes 6291460
